TPU v7x, 256 devices: a whole 4x4x8 slice. The times are simulated.
256 devices in a mesh: sp: 64 (over z, x, core), tp: 4 (over y).
Axes of the slice: x: 4, y: 4, z: 8, core: 2. Of those that a mesh axis runs over, the one named last changes fastest.
Arguments:
- resid: bfloat16 [16384, 4096], P(('sp', 'tp')), may hold values from -6 to 6
- queries: bfloat16 [16384, 2048], P('sp', 'tp'), may hold values from -6 to 6
- keys: bfloat16 [16384, 512], P('sp', 'tp'), may hold values from -6 to 6
- values: bfloat16 [16384, 512], P('sp', 'tp'), may hold values from -6 to 6
- q_gain: float32 [128], replicated, may hold values from 0.5 to 6
- key_norm_gain: float32 [128], replicated, may hold values from 0.5 to 6
- out_weight: bfloat16 [2048, 4096], P('tp'), may hold values from -0.125 to 0.125
- norm1_gain: float32 [4096], replicated, may hold values from 0.1 to 1.9
- norm2_gain: float32 [4096], replicated, may hold values from 0.1 to 1.9
- expert_ids: int32 [16384, 2], P(('sp', 'tp')), may hold values from 0 to 63, all different within a row; in each aligned block of 64 rows (0 to 63, 64 to 127, ...) at most 3 rows name the same one
- group_weight: float32 [16384], P(('sp', 'tp')), may hold values from 0.3 to 1
- expert_weight: float32 [16384, 2], P(('sp', 'tp')), may hold values from 0.1 to 1
- gate_proj: bfloat16 [64, 4096, 1024], P('sp', None, 'tp'), may hold values from -0.09375 to 0.09375
- up_proj: bfloat16 [64, 4096, 1024], P('sp', None, 'tp'), may hold values from -0.09375 to 0.09375
- down_proj: bfloat16 [64, 1024, 4096], P('sp', 'tp'), may hold values from -0.1875 to 0.1875
Outputs:
- mixed_out: bfloat16 [16384, 4096], P(('sp', 'tp'))
Inputs may be any that keep to these rules, and one draw needn't show every extreme that they name: `expert_ids`: each row names 2 different experts. Among the rows of one device (aligned blocks of 64 rows) no expert is named by more than 3 rows, a bound that some block reaches.
All inputs are finite; a program needn't handle non-finite values.
Results may differ from a plain program's by a relative error of at most 0.012.
The roundings to bfloat16 on the way count: a program that leaves them out, or rounds other values in their place, can miss the bound.
Values may be sent and summed in bfloat16 or wider, within the bound.
A program may use at most 192 MiB of HBM per device.

v0:
```python
import math

import jax
import jax.numpy as jnp
from jax import lax
from jax.sharding import PartitionSpec as P

GRID_W = 64


deep_alpha = 2.0**0.5
rope_theta = 10000.0


def in_one_piece(arrays, axis, dim, along):
    both = jnp.concatenate(arrays, axis=along)
    filled, at, gathered = (lax.all_gather(both, axis, axis=dim, tiled=True), 0, [])
    for a in arrays:
        gathered.append(lax.slice_in_dim(filled, at, at + a.shape[along], axis=along))
        at += a.shape[along]
    return tuple(gathered)


def copy_for_each(array, axis):
    devices = lax.axis_size(axis)
    return lax.all_to_all(
        jnp.broadcast_to(array[None], (devices, *array.shape)), axis, 0, 0, tiled=True
    )


def joined_along(parts, dim):
    lengths = list(parts.shape[1:])
    lengths[dim] *= parts.shape[0]
    return jnp.moveaxis(parts, 0, dim).reshape(lengths)


def collect(array, axis, dim):
    parts = copy_for_each(array, axis)
    return joined_along(parts, dim)


def cut_along(array, dim, devices):
    lengths = array.shape
    parts = array.reshape(*lengths[:dim], devices, lengths[dim] // devices, *lengths[dim + 1 :])
    return jnp.moveaxis(parts, dim, 0)


def sent_and_summed(array, axis, dim):
    devices = lax.axis_size(axis)
    parts = lax.all_to_all(cut_along(array, dim, devices), axis, 0, 0, tiled=True)
    return jnp.sum(parts.astype(jnp.float32), axis=0)


def apply_rotary_heads(block, gain, grid_positions):
    values32 = block.astype(jnp.float32)
    normed = values32 * lax.rsqrt(jnp.mean(values32 * values32, -1, keepdims=True) + 1e-06) * gain
    half = normed.shape[-1] // 2
    inv_freq = rope_theta ** (-jnp.arange(0, half, 2, dtype=jnp.float32) / half)
    grid_row = (grid_positions // GRID_W).astype(jnp.float32)
    grid_col = (grid_positions % GRID_W).astype(jnp.float32)
    angle = jnp.concatenate([grid_row[:, None] * inv_freq, grid_col[:, None] * inv_freq], -1)[
        :, None, :
    ]
    cosine = jnp.cos(angle)
    sine = jnp.sin(angle)
    first = normed[..., :half]
    second = normed[..., half:]
    turned = jnp.concatenate([first * cosine - second * sine, first * sine + second * cosine], -1)
    return turned.astype(jnp.bfloat16)


def layer_norm_gain(summed, gain):
    centre = summed - jnp.mean(summed, -1, keepdims=True)
    spread = jnp.mean(centre * centre, -1, keepdims=True)
    return centre * lax.rsqrt(spread + 1e-06) * gain


def per_device(
    resid,
    queries,
    keys,
    values,
    q_gain,
    key_norm_gain,
    out_weight,
    norm1_gain,
    norm2_gain,
    expert_ids,
    group_weight,
    expert_weight,
    gate_proj,
    up_proj,
    down_proj,
):
    local_tokens = queries.shape[0]
    head_size = q_gain.shape[0]
    kv_local = keys.shape[1] // head_size
    query_group = queries.shape[1] // head_size // kv_local
    model_width = resid.shape[1]
    score_scale = head_size ** (-0.5)
    grid_positions = lax.axis_index("sp") * local_tokens + jnp.arange(local_tokens, dtype=jnp.int32)
    q_rot = apply_rotary_heads(
        queries.reshape(local_tokens, kv_local * query_group, head_size), q_gain, grid_positions
    )
    query_head_rows = q_rot.reshape(local_tokens, kv_local, query_group, head_size).transpose(
        1, 2, 0, 3
    )
    query_head_rows = query_head_rows.reshape(kv_local, query_group * local_tokens, head_size)
    rotated_keys = apply_rotary_heads(
        keys.reshape(local_tokens, kv_local, head_size), key_norm_gain, grid_positions
    )
    rotated_keys = rotated_keys.reshape(local_tokens, kv_local * head_size)
    start_state = (
        jnp.full((kv_local, query_group * local_tokens), -1e30, jnp.float32),
        jnp.zeros((kv_local, query_group * local_tokens), jnp.float32),
        jnp.zeros((kv_local, query_group * local_tokens, head_size), jnp.float32),
    )
    key_piece, value_piece = in_one_piece((rotated_keys, values), "sp", 0, 1)
    length = key_piece.shape[0]
    span = math.gcd(length, 512)
    key_blocks = key_piece.reshape(length // span, span, kv_local, head_size)
    value_blocks = value_piece.reshape(length // span, span, kv_local, head_size)

    def inner(state, blocks):
        row_max, row_sum, weighted = state
        key_tile, value_block = blocks
        scores = (
            jnp.einsum(
                "pmw,fpw->pmf", query_head_rows, key_tile, preferred_element_type=jnp.float32
            )
            * score_scale
        )
        new_max = jnp.maximum(row_max, jnp.max(scores, -1))
        shrink_old = jnp.exp(row_max - new_max)
        probs = jnp.exp(scores - new_max[..., None])
        row_sum = row_sum * shrink_old + jnp.sum(probs, -1)
        weighted = weighted * shrink_old[..., None] + jnp.einsum(
            "wno,ows->wns",
            probs.astype(jnp.bfloat16),
            value_block,
            preferred_element_type=jnp.float32,
        )
        return ((new_max, row_sum, weighted), None)

    state, _ = lax.scan(inner, start_state, (key_blocks, value_blocks))
    row_max, row_sum, weighted = state
    attn = (weighted / row_sum[..., None]).astype(jnp.bfloat16)
    attn = attn.reshape(kv_local, query_group, local_tokens, head_size).transpose(2, 0, 1, 3)
    attn = attn.reshape(local_tokens, kv_local * query_group * head_size)
    lanes = lax.axis_size("tp")
    own_rows = local_tokens // lanes
    merged = lax.all_to_all(attn, "tp", split_axis=0, concat_axis=1, tiled=True)
    proj = jnp.dot(merged, collect(out_weight, "tp", 0), preferred_element_type=jnp.float32)
    proj = proj.astype(jnp.bfloat16)
    summed = deep_alpha * resid.astype(jnp.float32) + proj.astype(jnp.float32)
    x_one = layer_norm_gain(summed, norm1_gain).astype(jnp.bfloat16)
    top_count = expert_ids.shape[1]
    sp_count = lax.axis_size("sp")
    expert_local = gate_proj.shape[0]
    expert_total = expert_local * sp_count
    capacity = (3 * top_count * own_rows + 2 * expert_total - 1) // (2 * expert_total)
    flat_ids = expert_ids.reshape(-1)
    one_hot = (flat_ids[:, None] == jnp.arange(expert_total, dtype=jnp.int32)[None, :]).astype(
        jnp.int32
    )
    earlier = jnp.cumsum(one_hot, 0) - one_hot
    rank = jnp.sum(earlier * one_hot, 1)
    slot = flat_ids * capacity + rank
    placing = slot[:, None] == jnp.arange(expert_total * capacity, dtype=jnp.int32)[None, :]
    placing = placing.astype(jnp.bfloat16).reshape(own_rows, top_count, expert_total * capacity)
    placing = jnp.sum(placing, 1)
    outgoing = lax.dot_general(
        placing, x_one, (((0,), (0,)), ((), ())), preferred_element_type=jnp.float32
    ).astype(jnp.bfloat16)
    outgoing = outgoing.reshape(expert_total, capacity, model_width)
    received = lax.all_to_all(outgoing, "sp", split_axis=0, concat_axis=0, tiled=True)
    arrived = received.reshape(sp_count, expert_local, capacity, model_width).transpose(0, 2, 1, 3)
    arrived = arrived.reshape(sp_count * capacity, expert_local, model_width)
    piece = lax.all_gather(arrived, "tp", axis=0, tiled=True)
    gate_part = jnp.einsum("red,edf->ref", piece, gate_proj, preferred_element_type=jnp.float32)
    up_part = jnp.einsum("red,edf->ref", piece, up_proj, preferred_element_type=jnp.float32)
    hidden = (jax.nn.silu(gate_part) * up_part).astype(jnp.bfloat16)
    partial_sum = jnp.einsum("ref,efd->red", hidden, down_proj, preferred_element_type=jnp.float32)
    rounded = lax.optimization_barrier(partial_sum.astype(jnp.bfloat16))
    expert_out = sent_and_summed(rounded.astype(jnp.float32).astype(jnp.bfloat16), "tp", 0).astype(
        jnp.bfloat16
    )
    returning = expert_out.reshape(sp_count, capacity, expert_local, model_width).transpose(
        0, 2, 1, 3
    )
    returning = returning.reshape(sp_count * expert_local, capacity, model_width)
    returned = lax.all_to_all(returning, "sp", split_axis=0, concat_axis=0, tiled=True)
    returned = returned.reshape(expert_total * capacity, model_width)
    picked_out = returned[slot].reshape(own_rows, top_count, model_width)
    gates = group_weight[:, None] * expert_weight / jnp.sum(expert_weight, -1, keepdims=True)
    moe = jnp.sum(gates[..., None] * picked_out.astype(jnp.float32), 1)
    final = deep_alpha * x_one.astype(jnp.float32) + moe
    return layer_norm_gain(final, norm2_gain).astype(jnp.bfloat16)


def solution(mesh):
    in_specs = (
        P(("sp", "tp"), None),
        P("sp", "tp"),
        P("sp", "tp"),
        P("sp", "tp"),
        P(),
        P(),
        P("tp", None),
        P(),
        P(),
        P(("sp", "tp"), None),
        P(("sp", "tp")),
        P(("sp", "tp"), None),
        P("sp", None, "tp"),
        P("sp", None, "tp"),
        P("sp", "tp", None),
    )
    out_specs = P(("sp", "tp"), None)
    return jax.shard_map(
        per_device, mesh=mesh, in_specs=in_specs, out_specs=out_specs, check_vma=False
    )
```

profile of v0, /device:TPU:2, one launch (start us, length us, event | category | flops | bytes accessed | tf_op | source)
XLA Modules:
  0.0 655.9 jit_solution(16270576752289159782)
XLA Ops:
  11.0 7.5 %broadcast_in_dim.11 = bf16[4,512,4096]{2,1,0:T(8,128)(2,1)} broadcast(bf16[512,4096]{1,0:T(8,128)(2,1)} %param.23), dimensions={1,2} | broadcast | bytes 20971520 | tf_op jit(solution)/shard_map/broadcast_in_dim | solution.py:27
  18.5 7.0 %all-to-all-start.1 = ((bf16[4,512,4096]{2,1,0:T(8,128)(2,1)}), bf16[4,512,4096]{2,1,0:T(8,128)(2,1)}, u32[]{:S(2)}, u32[]{:S(2)}) async-start(bf16[4,512,4096]{2,1,0:T(8,128)(2,1)} %broadcast_in_dim.11), calls=%async_computation.1 | async-start | bytes 33554432 | tf_op jit(solution)/shard_map/all_to_all | solution.py:26
  29.7 66.1 %all-gather.3.cloned.1.call-done = bf16[16384,256]{1,0:T(8,128)(2,1)} async-done(((bf16[256,256]{1,0:T(8,128)(2,1)}), bf16[16384,256]{1,0:T(8,128)(2,1)}) %all-gather.3.cloned.1.call-update) | async-done | bytes 8388624 | tf_op jit(solution)/shard_map/all_gather | solution.py:17
  95.8 5.7 fusion.86
  101.5 206.1 %while.15 = (s32[]{:T(128)}, f32[1,1024]{1,0:T(1,128)S(1)}, f32[1,1024]{1,0:T(1,128)S(1)}, f32[1,1024,128]{2,1,0:T(8,128)S(1)}, bf16[32,512,1,128]{3,1,2,0:T(8,1...) while((s32[]{:T(128)}, f32[1,1024]{1,0:T(1,128)S(1)}, ...), condition=%wide.region_5.6_spmd.clone, body=%wide.region_2.5_spmd.clone.sunk | while | flops 273028096 | bytes 16319621 | solution.py:145
  120.8 2.7 multiply_reduce_fusion.6
  127.2 2.7 multiply_reduce_fusion.6
  133.7 2.7 multiply_reduce_fusion.6
  140.1 2.7 multiply_reduce_fusion.6
  146.5 2.7 multiply_reduce_fusion.6
  153.0 2.7 multiply_reduce_fusion.6
  159.4 2.7 multiply_reduce_fusion.6
  165.9 2.7 multiply_reduce_fusion.6
  172.3 2.7 multiply_reduce_fusion.6
  178.8 2.7 multiply_reduce_fusion.6
  185.2 2.7 multiply_reduce_fusion.6
  191.6 2.7 multiply_reduce_fusion.6
  198.1 2.7 multiply_reduce_fusion.6
  204.5 2.7 multiply_reduce_fusion.6
  211.0 2.7 multiply_reduce_fusion.6
  217.4 2.7 multiply_reduce_fusion.6
  223.9 2.7 multiply_reduce_fusion.6
  230.3 2.7 multiply_reduce_fusion.6
  236.7 2.7 multiply_reduce_fusion.6
  243.2 2.7 multiply_reduce_fusion.6
  249.6 2.7 multiply_reduce_fusion.6
  268.9 2.7 multiply_reduce_fusion.6
  275.4 2.7 multiply_reduce_fusion.6
  294.7 2.7 multiply_reduce_fusion.6
  301.2 2.7 multiply_reduce_fusion.6
  308.8 4.3 all-to-all-start
  313.3 6.9 %all-to-all-done = bf16[4,64,512]{2,1,0:T(8,128)(2,1)S(1)} async-done(((bf16[4,64,512]{2,1,0:T(8,128)(2,1)}), bf16[4,64,512]{2,1,0:T(8,128)(2,1)S(1)}, u32[]{:S(2)}, u32[]{:S(2)}) %all-to-all-start) | async-done | bytes 262176 | tf_op jit(solution)/shard_map/all_to_all | solution.py:152
  320.2 9.0 %fusion.87 = (f32[64]{0:T(128)S(1)}, f32[64,4096]{1,0:T(8,128)S(1)}) fusion(bf16[4,512,4096]{2,1,0:T(8,128)(2,1)} %all-to-all-done.1, bf16[4,64,512]{2,1,0:T(8,128)(2,1)S(1)} %all-to-all-done, bf16[64,4096]{1,0:T(8,128)(2,1)} %param.17), kind=kOutput, calls=%fused_computation.117 | convolution fusion | flops 1075314688 | bytes 18612480 | tf_op jit(solution)/shard_map/dot_general | solution.py:153
  331.3 4.1 reshape.420
  335.4 58.7 %all_to_all.36 = bf16[64,3,4096]{2,1,0:T(4,128)(2,1)} all-to-all(bf16[64,3,4096]{2,1,0:T(4,128)(2,1)} %reshape.420), channel_id=1, replica_groups=mesh['sp'=64,'tp'=4] {'sp'}, dimensions={0} | all-to-all | bytes 3145728 | tf_op jit(solution)/shard_map/all_to_all | solution.py:176
  394.0 4.3 reshape_transpose_reshape.6
  398.3 62.7 %all-gather.5.cloned.1.call-done = bf16[768,1,4096]{2,0,1:T(8,128)(2,1)} async-done(((bf16[192,1,4096]{2,0,1:T(8,128)(2,1)}), bf16[768,1,4096]{2,0,1:T(8,128)(2,1)}) %all-gather.5.cloned.1.call-update) | async-done | bytes 6291472 | tf_op jit(solution)/shard_map/all_gather | solution.py:179
  461.0 6.1 fusion.29
  467.2 12.8 %fusion.22 = bf16[768,1,4096]{2,0,1:T(8,128)(2,1)} fusion(bf16[1,256,4096]{2,1,0:T(8,128)(2,1)S(1)} %copy-done, bf16[1,4096,256]{2,1,0:T(8,128)(2,1)} %param.30, bf16[768,1,4096]{2,0,1:T(8,128)(2,1)} %all-gather.5.cloned.1.call-done, f32[768,1,256]{2,0,1:T(8,128)} %fusion.29), kind=kOutput, calls=%fused_computation.30 | convolution fusion | flops 3225550848 | bytes 17563648 | tf_op jit(solution)/shard_map/ref,efd->red/dot_general | solution.py:183
  479.9 78.1 %all_to_all.37 = bf16[4,192,1,4096]{3,1,2,0:T(8,128)(2,1)} all-to-all(bf16[4,192,1,4096]{3,1,2,0:T(8,128)(2,1)} %bitcast.161), channel_id=1, replica_groups=mesh['sp'=64,'tp'=4] {'tp'}, dimensions={0} | all-to-all | bytes 12582912 | tf_op jit(solution)/shard_map/all_to_all | solution.py:50
  558.1 5.6 reduce_sum.128
  563.6 4.1 reshape_transpose_reshape.7
  567.7 10.9 %all-to-all-start.4 = ((bf16[64,3,4096]{2,1,0:T(4,128)(2,1)}), bf16[64,3,4096]{2,1,0:T(4,128)(2,1)}, u32[]{:S(2)}, u32[]{:S(2)}) async-start(bf16[64,3,4096]{2,1,0:T(4,128)(2,1)} %reshape_transpose_reshape.7), calls=%async_computation.4 | async-start | bytes 4194304 | tf_op jit(solution)/shard_map/all_to_all | solution.py:192
  578.9 50.8 %all-to-all-done.4 = bf16[64,3,4096]{2,1,0:T(4,128)(2,1)} async-done(((bf16[64,3,4096]{2,1,0:T(4,128)(2,1)}), bf16[64,3,4096]{2,1,0:T(4,128)(2,1)}, u32[]{:S(2)}, u32[]{:S(2)}) %all-to-all-start.4) | async-done | bytes 1572896 | tf_op jit(solution)/shard_map/all_to_all | solution.py:192
  629.8 4.3 reshape.427
  634.0 4.8 gather_fusion
  638.8 3.4 reshape.429
  642.2 4.8 multiply_reduce_fusion.1
  (296 shorter events, 153.0 us)
Async XLA Ops:
  6.5 460.6 %copy-start = (bf16[1,256,4096]{2,1,0:T(8,128)(2,1)S(1)}, bf16[1,256,4096]{2,1,0:T(8,128)(2,1)}, u32[]{:S(2)}) copy-start(bf16[1,256,4096]{2,1,0:T(8,128)(2,1)} %param.31) | copy-start | bytes 6291460
  6.5 89.2 %all-gather.3.cloned.1.call-start = ((), (), s32[]{:S(2)}) async-start(), calls=%async_computation.5 | async-start | bytes 8519680 | tf_op jit(solution)/shard_map/all_gather | solution.py:17
  18.5 290.4 %all-to-all-start.1 = ((bf16[4,512,4096]{2,1,0:T(8,128)(2,1)}), bf16[4,512,4096]{2,1,0:T(8,128)(2,1)}, u32[]{:S(2)}, u32[]{:S(2)}) async-start(bf16[4,512,4096]{2,1,0:T(8,128)(2,1)} %broadcast_in_dim.11), calls=%async_computation.1 | async-start | bytes 33554432 | tf_op jit(solution)/shard_map/all_to_all | solution.py:26
  25.4 2.1 copy-start.6
  27.5 1.3 copy-start.5
  104.1 2.2 copy-start.1
  110.6 2.2 copy-start.1
  117.0 2.2 copy-start.1
  123.4 2.2 copy-start.1
  129.9 2.2 copy-start.1
  136.3 2.2 copy-start.1
  142.8 2.2 copy-start.1
  149.2 2.2 copy-start.1
  155.7 2.2 copy-start.1
  162.1 2.2 copy-start.1
  168.5 2.2 copy-start.1
  175.0 2.2 copy-start.1
  181.4 2.2 copy-start.1
  187.9 2.2 copy-start.1
  194.3 2.2 copy-start.1
  200.7 2.2 copy-start.1
  207.2 2.2 copy-start.1
  213.6 2.2 copy-start.1
  220.1 2.2 copy-start.1
  226.5 2.2 copy-start.1
  233.0 2.2 copy-start.1
  239.4 2.2 copy-start.1
  245.8 2.2 copy-start.1
  252.3 2.2 copy-start.1
  258.7 2.2 copy-start.1
  265.2 2.2 copy-start.1
  271.6 2.2 copy-start.1
  278.1 2.2 copy-start.1
  284.5 2.2 copy-start.1
  290.9 2.2 copy-start.1
  297.4 2.2 copy-start.1
  303.8 2.2 copy-start.1
  308.8 11.4 %all-to-all-start = ((bf16[4,64,512]{2,1,0:T(8,128)(2,1)}), bf16[4,64,512]{2,1,0:T(8,128)(2,1)S(1)}, u32[]{:S(2)}, u32[]{:S(2)}) async-start(bf16[4,64,512]{2,1,0:T(8,128)(2,1)} %all_to_all.24), calls=%async_computation | async-start | bytes 524288 | tf_op jit(solution)/shard_map/all_to_all | solution.py:152
  313.1 147.9 %all-gather.5.cloned.1.call-start = ((), (), s32[]{:S(2)}) async-start(), calls=%async_computation.6 | async-start | bytes 7864320 | tf_op jit(solution)/shard_map/all_gather | solution.py:179
  313.3 16.2 %copy-start.2 = (f32[4096]{0:T(1024)S(1)}, f32[4096]{0:T(1024)}, u32[]{:S(2)}) copy-start(f32[4096]{0:T(1024)} %param.24) | copy-start | bytes 49156
  567.7 11.0 %copy-start.4 = (f32[64,2]{0,1:T(2,128)S(1)}, f32[64,2]{0,1:T(2,128)}, u32[]{:S(2)}) copy-start(f32[64,2]{0,1:T(2,128)} %param.28) | copy-start | bytes 1540
  567.7 11.1 %copy-start.7 = (f32[64]{0:T(128)S(1)}, f32[64]{0:T(128)}, u32[]{:S(2)}) copy-start(f32[64]{0:T(128)} %param.27) | copy-start | bytes 772
  567.7 62.0 %all-to-all-start.4 = ((bf16[64,3,4096]{2,1,0:T(4,128)(2,1)}), bf16[64,3,4096]{2,1,0:T(4,128)(2,1)}, u32[]{:S(2)}, u32[]{:S(2)}) async-start(bf16[64,3,4096]{2,1,0:T(4,128)(2,1)} %reshape_transpose_reshape.7), calls=%async_computation.4 | async-start | bytes 4194304 | tf_op jit(solution)/shard_map/all_to_all | solution.py:192
  647.0 0.9 copy-start.3
Sparse Core Ops, SparseCore 0:
  11.1 84.6 all-gather.2
  398.4 62.5 all-gather.4
where the time goes:
time: 658 us; the launch traced here: 656 us
  waiting for transfers between devices  187 us (28%)
  matrix products  164 us (25%)
  blocking collectives  137 us (21%)
  other arithmetic  88.6 us (13%)
  local copies, waits for them, and re-layouts  43.4 us (7%)
  starting transfers between devices  22.1 us (3%)
  between operations  13.7 us (2%)
    dot_general x32, matrix products, inner(): jnp.einsum('pmw,fpw->pmf', query_head_rows, key_tile, preferred_element_t...  85.1 us
    all_to_all x1, blocking collectives, sent_and_summed(): lax.all_to_all(cut_along(array, dim, devices), axis, 0, 0, tiled=True)  78.1 us
    reduce_sum x32, other arithmetic, inner(): row_sum = row_sum * shrink_old + jnp.sum(probs, -1)  67.6 us
    all_gather x1, waiting for transfers between devices, in_one_piece(): lax.all_gather(both, axis, axis=dim, tiled=True)  66.1 us
    all_gather x1, waiting for transfers between devices, per_device(): piece = lax.all_gather(arrived, 'tp', axis=0, tiled=True)  62.7 us
    all_to_all x1, blocking collectives, per_device(): lax.all_to_all(outgoing, 'sp', split_axis=0, concat_axis=0, tiled=True)  58.7 us
    all_to_all x1, waiting for transfers between devices, per_device(): lax.all_to_all(returning, 'sp', split_axis=0, concat_axis=0, tiled=True)  50.8 us
    dot_general x32, matrix products, inner(): jnp.einsum('wno,ows->wns', probs.astype(jnp.bfloat16), value_block, prefe...  49 us
  transfers between devices with their start and end apart: 5, of which 4 were waited for; matrix products, arithmetic and copies ran while one was open for 34% of the time, Pallas kernels for 0%

commit v1 on v0

v1 whole, which is shorter than its diff:
```python
import jax
import jax.numpy as jnp
import numpy as np
from jax import lax
from jax.experimental import pallas as pl
from jax.experimental.pallas import tpu as pltpu
from jax.sharding import PartitionSpec as P

GRID_W = 64
CAP = 3
KEY_BLOCK = 1024
QUERY_TILE = 512

deep_alpha = 2.0**0.5
rope_theta = 10000.0
VMEM_LIMIT = 60 * 1024 * 1024


def apply_rotary_heads(block, gain, grid_positions):
    values32 = block.astype(jnp.float32)
    normed = values32 * lax.rsqrt(jnp.mean(values32 * values32, -1, keepdims=True) + 1e-06) * gain
    half = normed.shape[-1] // 2
    inv_freq = rope_theta ** (-jnp.arange(0, half, 2, dtype=jnp.float32) / half)
    grid_row = (grid_positions // GRID_W).astype(jnp.float32)
    grid_col = (grid_positions % GRID_W).astype(jnp.float32)
    angle = jnp.concatenate([grid_row[:, None] * inv_freq, grid_col[:, None] * inv_freq], -1)[
        :, None, :
    ]
    cosine = jnp.cos(angle)
    sine = jnp.sin(angle)
    first = normed[..., :half]
    second = normed[..., half:]
    turned = jnp.concatenate([first * cosine - second * sine, first * sine + second * cosine], -1)
    return turned.astype(jnp.bfloat16)


def attention_kernel(qt_ref, k_ref, v_ref, o_ref, m_ref, l_ref, acc_ref):
    step = pl.program_id(0)
    rows = qt_ref.shape[1]
    width = v_ref.shape[1]
    heads = o_ref.shape[1] // width
    tokens = o_ref.shape[0]

    @pl.when(step == 0)
    def _():
        m_ref[...] = jnp.full_like(m_ref, -1e30)
        l_ref[...] = jnp.zeros_like(l_ref)
        acc_ref[...] = jnp.zeros_like(acc_ref)

    k = k_ref[...]
    k_twice = jnp.concatenate([k, k], 1)
    v_t = v_ref[...].T
    tile = min(QUERY_TILE, rows)
    count = rows // tile

    def scores(t):
        return jnp.dot(
            k_twice, qt_ref[:, t * tile : (t + 1) * tile], preferred_element_type=jnp.float32
        )

    s = scores(0)
    for t in range(count):
        following = scores(t + 1) if t + 1 < count else None
        at = slice(t * tile, (t + 1) * tile)
        m_old = m_ref[:, at]
        m_new = jnp.maximum(m_old, jnp.max(s, 0, keepdims=True))
        shrink = jnp.exp2(m_old - m_new)
        p = jnp.exp2(s - m_new)
        l_ref[:, at] = l_ref[:, at] * shrink + jnp.sum(p, 0, keepdims=True)
        m_ref[:, at] = m_new
        pv = jnp.dot(v_t, p.astype(jnp.bfloat16), preferred_element_type=jnp.float32)
        acc_ref[:, at] = acc_ref[:, at] * shrink + pv
        s = following

    @pl.when(step == pl.num_programs(0) - 1)
    def _():
        for h in range(heads):
            at = slice(h * tokens, (h + 1) * tokens)
            out = acc_ref[:, at] / l_ref[:, at]
            o_ref[:, h * width : (h + 1) * width] = out.T.astype(jnp.bfloat16)


def attention(q_t, keys_values, tokens, width):
    length = keys_values.shape[0]
    rows = q_t.shape[1]
    block = min(KEY_BLOCK, length)
    heads = rows // tokens
    return pl.pallas_call(
        attention_kernel,
        grid=(length // block,),
        in_specs=[
            pl.BlockSpec(q_t.shape, lambda i: (0, 0)),
            pl.BlockSpec((block, width), lambda i: (i, 0)),
            pl.BlockSpec((block, width), lambda i: (i, 1)),
        ],
        out_specs=pl.BlockSpec((tokens, heads * width), lambda i: (0, 0)),
        out_shape=jax.ShapeDtypeStruct((tokens, heads * width), jnp.bfloat16),
        scratch_shapes=[
            pltpu.VMEM((1, rows), jnp.float32),
            pltpu.VMEM((1, rows), jnp.float32),
            pltpu.VMEM((width, rows), jnp.float32),
        ],
        compiler_params=pltpu.CompilerParams(vmem_limit_bytes=VMEM_LIMIT),
        cost_estimate=pl.CostEstimate(
            flops=4 * rows * length * width,
            bytes_accessed=length * width * 4,
            transcendentals=rows * length,
        ),
        name="attention",
    )(q_t, keys_values, keys_values)


def gate_up_kernel(x_ref, wg_ref, wu_ref, h_ref):
    parts, _, depth = x_ref.shape
    gate = None
    up = None
    for j in range(parts):
        x = x_ref[j]
        g = jnp.dot(x, wg_ref[j * depth : (j + 1) * depth, :], preferred_element_type=jnp.float32)
        u = jnp.dot(x, wu_ref[j * depth : (j + 1) * depth, :], preferred_element_type=jnp.float32)
        gate = g if gate is None else gate + g
        up = u if up is None else up + u
    h_ref[...] = (gate / (1.0 + jnp.exp(-gate)) * up).astype(jnp.bfloat16)


def gate_up(x, w_gate, w_up):
    parts, rows, depth = x.shape
    hidden = w_gate.shape[1]
    block = rows // 4
    return pl.pallas_call(
        gate_up_kernel,
        grid=(rows // block,),
        in_specs=[
            pl.BlockSpec((parts, block, depth), lambda i: (0, i, 0)),
            pl.BlockSpec(w_gate.shape, lambda i: (0, 0)),
            pl.BlockSpec(w_up.shape, lambda i: (0, 0)),
        ],
        out_specs=pl.BlockSpec((block, hidden), lambda i: (i, 0)),
        out_shape=jax.ShapeDtypeStruct((rows, hidden), jnp.bfloat16),
        compiler_params=pltpu.CompilerParams(vmem_limit_bytes=VMEM_LIMIT),
        cost_estimate=pl.CostEstimate(
            flops=4 * rows * parts * depth * hidden,
            bytes_accessed=2 * parts * depth * (rows + 2 * hidden),
            transcendentals=rows * hidden,
        ),
        name="gate_up",
    )(x, w_gate, w_up)


def down_kernel(h_ref, w_ref, o_ref):
    parts, _, depth = h_ref.shape
    total = None
    for j in range(parts):
        part = jnp.dot(
            h_ref[j], w_ref[j * depth : (j + 1) * depth, :], preferred_element_type=jnp.float32
        )
        part = part.astype(jnp.bfloat16).astype(jnp.float32)
        total = part if total is None else total + part
    o_ref[...] = total.astype(jnp.bfloat16)


def down(h, w):
    parts, rows, depth = h.shape
    width = w.shape[1]
    block = rows // 4
    return pl.pallas_call(
        down_kernel,
        grid=(rows // block,),
        in_specs=[
            pl.BlockSpec((parts, block, depth), lambda i: (0, i, 0)),
            pl.BlockSpec(w.shape, lambda i: (0, 0)),
        ],
        out_specs=pl.BlockSpec((block, width), lambda i: (i, 0)),
        out_shape=jax.ShapeDtypeStruct((rows, width), jnp.bfloat16),
        compiler_params=pltpu.CompilerParams(vmem_limit_bytes=VMEM_LIMIT),
        cost_estimate=pl.CostEstimate(
            flops=2 * rows * parts * depth * width,
            bytes_accessed=2 * parts * depth * (rows + width) + 2 * rows * width,
            transcendentals=0,
        ),
        name="down",
    )(h, w)


def split_layer_norm(z, gain):
    local = z.shape[-1]
    mean = jnp.mean(z, -1)
    centre = z - mean[:, None]
    m2 = jnp.sum(centre * centre, -1)
    both = lax.all_gather(jnp.stack([mean, m2]), "tp", axis=0, tiled=False)
    means, m2s = both[:, 0], both[:, 1]
    full_mean = jnp.mean(means, 0)
    away = means - full_mean[None]
    spread = (jnp.sum(m2s, 0) + local * jnp.sum(away * away, 0)) / (local * both.shape[0])
    return (z - full_mean[:, None]) * lax.rsqrt(spread + 1e-06)[:, None] * gain


def per_device(
    resid,
    queries,
    keys,
    values,
    q_gain,
    key_norm_gain,
    out_weight,
    norm1_gain,
    norm2_gain,
    expert_ids,
    group_weight,
    expert_weight,
    gate_proj,
    up_proj,
    down_proj,
):
    tokens = queries.shape[0]
    width = q_gain.shape[0]
    heads = queries.shape[1] // width
    lanes = lax.axis_size("tp")
    sp_count = lax.axis_size("sp")
    lane = lax.axis_index("tp")
    own = tokens // lanes
    model_width = resid.shape[1]
    part = model_width // lanes

    positions = lax.axis_index("sp") * tokens + jnp.arange(tokens, dtype=jnp.int32)
    rotated_keys = apply_rotary_heads(keys.reshape(tokens, 1, width), key_norm_gain, positions)
    both = jnp.concatenate([rotated_keys.reshape(tokens, width), values], 1)
    keys_values = lax.all_gather(both, "sp", axis=0, tiled=True)

    out_slice = lax.all_to_all(out_weight, "tp", split_axis=1, concat_axis=0, tiled=True)
    down_slice = lax.all_to_all(down_proj[0], "tp", split_axis=1, concat_axis=0, tiled=True)
    resid_slice = lax.all_to_all(resid, "tp", split_axis=1, concat_axis=0, tiled=True)
    ids = lax.all_gather(expert_ids, "tp", axis=0, tiled=True)
    gates_own = (
        group_weight[:, None] * expert_weight / jnp.sum(expert_weight, -1, keepdims=True)
    )
    gates = lax.all_gather(gates_own, "tp", axis=0, tiled=True)

    q_rot = apply_rotary_heads(queries.reshape(tokens, heads, width), q_gain, positions)
    factor = np.float32(np.log2(np.e) * width**-0.5)
    scaled = q_rot.astype(jnp.float32) * factor
    coarse = lax.reduce_precision(scaled, 8, 7)
    fine = (scaled - coarse).astype(jnp.bfloat16)
    pair = jnp.concatenate([coarse.astype(jnp.bfloat16), fine], -1)
    q_t = pair.transpose(2, 1, 0).reshape(2 * width, heads * tokens)
    attn = attention(q_t, keys_values, tokens, width)
    attn = lax.all_gather(attn, "tp", axis=1, tiled=True)

    proj = jnp.dot(attn, out_slice, preferred_element_type=jnp.float32)
    proj = lax.reduce_precision(proj, 8, 7)
    summed = deep_alpha * resid_slice.astype(jnp.float32) + proj
    gain_one = lax.dynamic_slice_in_dim(norm1_gain, lane * part, part)
    gain_two = lax.dynamic_slice_in_dim(norm2_gain, lane * part, part)
    x_one = split_layer_norm(summed, gain_one).astype(jnp.bfloat16)

    top = ids.shape[1]
    per_expert = lanes * CAP
    blocks = ids.reshape(lanes, own * top)
    one_hot = (blocks[:, :, None] == jnp.arange(sp_count, dtype=jnp.int32)).astype(jnp.int32)
    earlier = jnp.cumsum(one_hot, 1) - one_hot
    rank = jnp.sum(earlier * one_hot, 2)
    slot = blocks * per_expert + jnp.arange(lanes, dtype=jnp.int32)[:, None] * CAP + rank
    slot = slot.reshape(tokens, top)
    slots = sp_count * per_expert
    chosen = slot[:, :, None] == jnp.arange(slots, dtype=jnp.int32)
    placing = jnp.any(chosen, 1).astype(jnp.bfloat16)
    outgoing = lax.dot_general(
        placing, x_one, (((0,), (0,)), ((), ())), preferred_element_type=jnp.float32
    ).astype(jnp.bfloat16)
    received = lax.all_to_all(
        outgoing.reshape(sp_count, per_expert, part), "sp", split_axis=0, concat_axis=0, tiled=True
    )
    gathered = lax.all_gather(received.reshape(slots, part), "tp", axis=0, tiled=False)
    hidden = gate_up(gathered, gate_proj[0], up_proj[0])
    hidden = lax.all_gather(hidden, "tp", axis=0, tiled=False)
    expert_out = down(hidden, down_slice)
    returned = lax.all_to_all(
        expert_out.reshape(sp_count, per_expert, part),
        "sp",
        split_axis=0,
        concat_axis=0,
        tiled=True,
    ).reshape(slots, part)
    weights = jnp.sum(jnp.where(chosen, gates[:, :, None], 0.0), 1)
    moe = None
    for _ in range(3):
        term = lax.reduce_precision(weights, 8, 7)
        weights = weights - term
        piece = jnp.dot(
            term.astype(jnp.bfloat16), returned, preferred_element_type=jnp.float32
        )
        moe = piece if moe is None else moe + piece
    final = deep_alpha * x_one.astype(jnp.float32) + moe
    mixed = split_layer_norm(final, gain_two).astype(jnp.bfloat16)
    return lax.all_to_all(mixed, "tp", split_axis=0, concat_axis=1, tiled=True)


def solution(mesh):
    in_specs = (
        P(("sp", "tp"), None),
        P("sp", "tp"),
        P("sp", "tp"),
        P("sp", "tp"),
        P(),
        P(),
        P("tp", None),
        P(),
        P(),
        P(("sp", "tp"), None),
        P(("sp", "tp")),
        P(("sp", "tp"), None),
        P("sp", None, "tp"),
        P("sp", None, "tp"),
        P("sp", "tp", None),
    )
    out_specs = P(("sp", "tp"), None)
    return jax.shard_map(
        per_device, mesh=mesh, in_specs=in_specs, out_specs=out_specs, check_vma=False
    )
```

time: 658 us -> 458 us (0.70)
  matrix products: 164 us -> 7.64 us
  other arithmetic: 88.6 us -> 8.92 us
  Pallas kernels: 0 us -> 41.1 us
  blocking collectives: 137 us -> 154 us
  waiting for transfers between devices: 187 us -> 176 us
  local copies, waits for them, and re-layouts: 43.4 us -> 33.7 us
    dot_general x67 -> x4, matrix products: 162 us -> 5.77 us  [the longest x1 3.85 us: per_device(): proj = jnp.dot(attn, out_slice, preferred_element_type=jnp.float32)]
    reduce_sum x39 -> x8, other arithmetic: 79.3 us -> 1.06 us  [the longest x2 0.51 us: split_layer_norm(): m2 = jnp.sum(centre * centre, -1)]
    pallas_call x0 -> x3, Pallas kernels: none -> 41.1 us  [the longest x1 27.7 us: attention(): pl.pallas_call(attention_kernel, grid=(length // block,), in_specs=[pl.Bl...]
    all_gather x0 -> x4, blocking collectives: none -> 38.7 us  [the longest x2 20.9 us: split_layer_norm(): both = lax.all_gather(jnp.stack([mean, m2]), 'tp', axis=0, tiled=False)]
    all_to_all x2 -> x3, blocking collectives: 137 us -> 116 us  [the longest x1 61.7 us: per_device(): lax.all_to_all(outgoing.reshape(sp_count, per_expert, part), 'sp', split_...]
    all_to_all x3, waiting for transfers between devices: 57.7 us -> 45.1 us  [the longest x1 42.6 us: per_device(): lax.all_to_all(expert_out.reshape(sp_count, per_expert, part), 'sp', spli...]
    all_to_all x1 -> x5, local copies, waits for them, and re-layouts: 0.8 us -> 12 us  [the longest x1 6.34 us: per_device(): lax.all_to_all(out_weight, 'tp', split_axis=1, concat_axis=0, tiled=True)]
    broadcast_in_dim x1 -> x0, local copies, waits for them, and re-layouts: 7.46 us -> none  [copy_for_each(): jnp.broadcast_to(array[None], (devices, *array.shape))]
  transfers between devices with their start and end apart: 5 -> 7, of which waited for: 4 -> 5; matrix products, arithmetic and copies ran while one was open for 34% -> 5% of each run, Pallas kernels for 0% -> 6%
where the time goes in v1:
time: 458 us; the launch traced here: 456 us
  waiting for transfers between devices  176 us (38%)
  blocking collectives  154 us (34%)
  Pallas kernels  41.1 us (9%)
  local copies, waits for them, and re-layouts  33.7 us (7%)
  starting transfers between devices  20.7 us (5%)
  between operations  13.5 us (3%)
  other arithmetic  8.92 us (2%)
  matrix products  7.64 us (2%)
    all_gather x1, waiting for transfers between devices, per_device(): lax.all_gather(received.reshape(slots, part), 'tp', axis=0, tiled=False)  63.7 us
    all_to_all x1, blocking collectives, per_device(): lax.all_to_all(outgoing.reshape(sp_count, per_expert, part), 'sp', split_...  61.7 us
    all_gather x1, waiting for transfers between devices, per_device(): keys_values = lax.all_gather(both, 'sp', axis=0, tiled=True)  61.1 us
    all_to_all x1, waiting for transfers between devices, per_device(): lax.all_to_all(expert_out.reshape(sp_count, per_expert, part), 'sp', spli...  42.6 us
    all_to_all x1, blocking collectives, per_device(): lax.all_to_all(down_proj[0], 'tp', split_axis=1, concat_axis=0, tiled=True)  42.4 us
    pallas_call x1, Pallas kernels, attention(): pl.pallas_call(attention_kernel, grid=(length // block,), in_specs=[pl.Bl...  27.7 us
    all_gather x2, blocking collectives, split_layer_norm(): both = lax.all_gather(jnp.stack([mean, m2]), 'tp', axis=0, tiled=False)  20.9 us
    all_to_all x1, blocking collectives, per_device(): return lax.all_to_all(mixed, 'tp', split_axis=0, concat_axis=1, tiled=True)  11.6 us
  transfers between devices with their start and end apart: 7, of which 5 were waited for; matrix products, arithmetic and copies ran while one was open for 5% of the time, Pallas kernels for 6%

profile of v1, /device:TPU:2, one launch (start us, length us, event | category | flops | bytes accessed | tf_op | source)
XLA Modules:
  0.0 456.3 jit_solution(2280250200840395297)
XLA Ops:
  6.6 1.0 fusion.9
  7.6 0.9 fusion.11
  8.7 0.6 fusion.12
  9.3 1.6 pad_maximum_fusion.3
  10.9 0.8 copy.97
  11.7 4.5 all-to-all-start
  16.4 6.5 %copy.78 = bf16[512,4096]{0,1:T(8,128)(2,1)} copy(bf16[512,4096]{1,0:T(8,128)(2,1)} %param.21) | data formatting | bytes 8388608 | tf_op args[6]
  22.9 0.3 multiply_reduce_fusion.2
  23.2 2.4 all-to-all-done
  25.7 5.1 %all-to-all-start.1 = ((bf16[512,4,1024]{0,2,1:T(8,128)(2,1)}), bf16[512,4,1024]{0,2,1:T(8,128)(2,1)}, u32[]{:S(2)}, u32[]{:S(2)}) async-start(bf16[512,4,1024]{0,2,1:T(8,128)(2,1)} %bitcast.68), calls=%async_computation.1 | async-start | bytes 8388608 | tf_op jit(solution)/shard_map/all_to_all | solution.py:230
  30.8 0.5 fusion.17
  31.4 0.3 multiply_multiply_fusion
  31.7 0.5 subtract_convert_fusion
  32.2 0.5 reduce-precision_convert_fusion.2
  32.7 0.3 maximum_bitcast_fusion
  33.0 0.6 copy.77
  33.7 0.9 copy.91
  34.6 61.1 %all-gather.12.cloned.1.call-done.k_ref.v_ref = bf16[16384,256]{1,0:T(8,128)(2,1)} async-done(((bf16[256,256]{1,0:T(8,128)(2,1)}), bf16[16384,256]{1,0:T(8,128)(2,1)}) %all-gather.12.cloned.1.call-update) | async-done | bytes 8388624 | tf_op jit(solution)/shard_map/all_gather | solution.py:228
  95.7 27.7 %attention.1 = bf16[256,512]{1,0:T(8,128)(2,1)} custom-call(bf16[256,1024]{1,0:T(8,128)(2,1)} %bitcast.76, bf16[16384,256]{1,0:T(8,128)(2,1)} %all-gather.12.cloned.1.call-done.k_ref.v_ref, bf16[16384,256]{1,0:T(8,128)(2,1)} %all-gather.12.cloned.1.call-done.k_ref.v_ref), custom_call_target="tpu_custom_call" | custom-call | flops 8589934592 | bytes 8388608 | tf_op jit(solution)/shard_map/attention/pallas_call | solution.py:88
  123.4 9.7 %all-gather.4 = s32[4,64,2]{1,2,0:T(2,128)S(1)} all-gather(s32[1,64,2]{1,2,0:T(2,128)S(1)} %bitcast.82), channel_id=1, replica_groups=mesh['sp'=64,'tp'=4] {'tp'}, dimensions={0}, use_global_device_ids=true | all-gather | bytes 2560 | tf_op jit(solution)/shard_map/all_gather | solution.py:233
  133.5 0.3 reduce_window_sum.11
  134.5 0.7 dynamic_slice.6
  135.5 6.3 %copy.79 = bf16[4,512,1024]{2,1,0:T(8,128)(2,1)} copy(bf16[4,512,1024]{1,2,0:T(8,128)(2,1)} %bitcast.9) | data formatting | bytes 8388608 | tf_op jit(solution)/shard_map/all_to_all | solution.py:230
  141.9 6.4 %all-gather.14.cloned.1.call-done = bf16[256,2048]{1,0:T(8,128)(2,1)} async-done(((bf16[256,512]{1,0:T(8,128)(2,1)}), bf16[256,2048]{1,0:T(8,128)(2,1)}) %all-gather.14.cloned.1.call-update) | async-done | bytes 1048592 | tf_op jit(solution)/shard_map/all_gather | solution.py:247
  148.2 3.8 fusion.27
  152.4 10.4 %all-gather.3 = f32[4,2,256]{2,1,0:T(2,128)S(1)} all-gather(f32[1,2,256]{2,1,0:T(2,128)S(1)} %maximum_bitcast_fusion.1), channel_id=2, replica_groups=mesh['sp'=64,'tp'=4] {'tp'}, dimensions={0}, use_global_device_ids=true | all-gather | bytes 10240 | tf_op jit(solution)/shard_map/all_gather | solution.py:190
  162.9 1.9 convolution_convert_fusion
  164.7 2.4 reshape.331
  167.1 61.7 %all_to_all.80 = bf16[64,12,1024]{2,1,0:T(8,128)(2,1)} all-to-all(bf16[64,12,1024]{2,1,0:T(8,128)(2,1)S(1)} %reshape.331), channel_id=1, replica_groups=mesh['sp'=64,'tp'=4] {'sp'}, dimensions={0} | all-to-all | bytes 3145728 | tf_op jit(solution)/shard_map/all_to_all | solution.py:270
  228.8 3.6 all_gather_reshape.3
  232.7 63.7 %all-gather.16.cloned.1.call-done.x_ref = bf16[4,768,1024]{2,1,0:T(8,128)(2,1)} async-done(((bf16[1,768,1024]{2,1,0:T(8,128)(2,1)}), bf16[4,768,1024]{2,1,0:T(8,128)(2,1)}) %all-gather.16.cloned.1.call-update) | async-done | bytes 6291472 | tf_op jit(solution)/shard_map/all_gather | solution.py:273
  296.4 8.0 %gate_up.1 = bf16[768,256]{1,0:T(8,128)(2,1)} custom-call(bf16[4,768,1024]{2,1,0:T(8,128)(2,1)} %all-gather.16.cloned.1.call-done.x_ref, bf16[4096,256]{1,0:T(8,128)(2,1)} %bitcast.83, bf16[4096,256]{1,0:T(8,128)(2,1)} %bitcast.84), custom_call_target="tpu_custom_call" | custom-call | flops 3221225472 | bytes 10485760 | tf_op jit(solution)/shard_map/gate_up/pallas_call | solution.py:130
  304.4 3.3 all_to_all.65
  307.7 0.6 copy.85
  308.3 42.4 %all_to_all.81 = bf16[256,4,1024]{2,0,1:T(8,128)(2,1)} all-to-all(bf16[256,4,1024]{2,0,1:T(8,128)(2,1)S(1)} %copy.85), channel_id=1, replica_groups=mesh['sp'=64,'tp'=4] {'tp'}, dimensions={1} | all-to-all | bytes 4194304 | tf_op jit(solution)/shard_map/all_to_all | solution.py:231
  350.7 5.5 %down.1 = bf16[768,1024]{1,0:T(8,128)(2,1)} custom-call(bf16[4,768,256]{2,1,0:T(8,128)(2,1)} %bitcast.85, bf16[1024,1024]{1,0:T(8,128)(2,1)} %bitcast.70), custom_call_target="tpu_custom_call" | custom-call | flops 1610612736 | bytes 5242880 | tf_op jit(solution)/shard_map/down/pallas_call | solution.py:166
  356.2 3.6 reshape.332
  359.8 10.9 %all-to-all-start.4 = ((bf16[64,12,1024]{2,1,0:T(8,128)(2,1)}), bf16[64,12,1024]{2,1,0:T(8,128)(2,1)}, u32[]{:S(2)}, u32[]{:S(2)}) async-start(bf16[64,12,1024]{2,1,0:T(8,128)(2,1)} %reshape.332), calls=%async_computation.4 | async-start | bytes 4194304 | tf_op jit(solution)/shard_map/all_to_all | solution.py:277
  370.7 8.1 %all-gather.5 = f32[4,64,2]{1,2,0:T(2,128)S(1)} all-gather(f32[1,64,2]{1,2,0:T(2,128)S(1)} %divide_bitcast_fusion), channel_id=1, replica_groups=mesh['sp'=64,'tp'=4] {'tp'}, dimensions={0}, use_global_device_ids=true | all-gather | bytes 2560 | tf_op jit(solution)/shard_map/all_gather | solution.py:237
  379.2 42.6 %all-to-all-done.4 = bf16[64,12,1024]{2,1,0:T(8,128)(2,1)} async-done(((bf16[64,12,1024]{2,1,0:T(8,128)(2,1)}), bf16[64,12,1024]{2,1,0:T(8,128)(2,1)}, u32[]{:S(2)}, u32[]{:S(2)}) %all-to-all-start.4) | async-done | bytes 1572896 | tf_op jit(solution)/shard_map/all_to_all | solution.py:277
  421.8 2.5 reshape.333
  424.3 0.6 fusion.7
  424.9 0.6 convolution_add_fusion.1
  425.5 0.8 fusion.28
  426.3 0.3 multiply_reduce_fusion
  426.6 10.4 %all-gather.6 = f32[4,2,256]{2,1,0:T(2,128)S(1)} all-gather(f32[1,2,256]{2,1,0:T(2,128)S(1)} %maximum_bitcast_fusion.2), channel_id=4, replica_groups=mesh['sp'=64,'tp'=4] {'tp'}, dimensions={0}, use_global_device_ids=true | all-gather | bytes 10240 | tf_op jit(solution)/shard_map/all_gather | solution.py:190
  437.3 11.6 %all_to_all.82 = bf16[4,64,1024]{2,1,0:T(8,128)(2,1)S(1)} all-to-all(bf16[4,64,1024]{2,1,0:T(8,128)(2,1)S(1)} %bitcast.71), channel_id=1, replica_groups=mesh['sp'=64,'tp'=4] {'tp'}, dimensions={0} | all-to-all | bytes 1048576 | tf_op jit(solution)/shard_map/all_to_all | solution.py:295
  448.9 0.8 copy.90
  (63 shorter events, 3.1 us)
Async XLA Ops:
  6.5 4.4 copy-start
  6.5 89.1 %all-gather.12.cloned.1.call-start = ((), (), s32[]{:S(2)}) async-start(), calls=%async_computation.6 | async-start | bytes 8519680 | tf_op jit(solution)/shard_map/all_gather | solution.py:228
  8.7 7.5 %copy-start.1 = (bf16[256,512]{1,0:T(8,128)(2,1)S(1)}, bf16[256,512]{1,0:T(8,128)(2,1)}, u32[]{:S(2)}) copy-start(bf16[256,512]{1,0:T(8,128)(2,1)} %param.16) | copy-start | bytes 786436
  11.7 13.9 %all-to-all-start = ((bf16[64,4,1024]{2,0,1:T(8,128)(2,1)}), bf16[64,4,1024]{2,0,1:T(8,128)(2,1)S(1)}, u32[]{:S(2)}, u32[]{:S(2)}) async-start(bf16[64,4,1024]{2,0,1:T(8,128)(2,1)} %bitcast.67), calls=%async_computation | async-start | bytes 1048576 | tf_op jit(solution)/shard_map/all_to_all | solution.py:232
  25.7 5.7 %copy-start.4 = (f32[128]{0:T(128)S(1)}, f32[128]{0:T(128)}, u32[]{:S(2)}) copy-start(f32[128]{0:T(128)} %param.19) | copy-start | bytes 1540
  25.7 109.8 %all-to-all-start.1 = ((bf16[512,4,1024]{0,2,1:T(8,128)(2,1)}), bf16[512,4,1024]{0,2,1:T(8,128)(2,1)}, u32[]{:S(2)}, u32[]{:S(2)}) async-start(bf16[512,4,1024]{0,2,1:T(8,128)(2,1)} %bitcast.68), calls=%async_computation.1 | async-start | bytes 8388608 | tf_op jit(solution)/shard_map/all_to_all | solution.py:230
  30.8 117.5 %all-gather.14.cloned.1.call-start = ((), (), s32[]{:S(2)}) async-start(), calls=%async_computation.7 | async-start | bytes 1310720 | tf_op jit(solution)/shard_map/all_gather | solution.py:247
  95.7 27.8 %copy-start.3 = (s32[64,2]{0,1:T(2,128)S(1)}, s32[64,2]{0,1:T(2,128)}, u32[]{:S(2)}) copy-start(s32[64,2]{0,1:T(2,128)} %param.24) | copy-start | bytes 1540
  123.4 173.0 %all-gather.16.cloned.1.call-start = ((), (), s32[]{:S(2)}) async-start(), calls=%async_computation.8 | async-start | bytes 7864320 | tf_op jit(solution)/shard_map/all_gather | solution.py:273
  232.4 118.3 %all-gather.18.cloned.1.call-start = ((), (), s32[]{:S(2)}) async-start(), calls=%async_computation.9 | async-start | bytes 1966080 | tf_op jit(solution)/shard_map/all_gather | solution.py:275
  359.8 10.9 %copy-start.2 = (f32[64,2]{0,1:T(2,128)S(1)}, f32[64,2]{0,1:T(2,128)}, u32[]{:S(2)}) copy-start(f32[64,2]{0,1:T(2,128)} %param.26) | copy-start | bytes 1540
  359.8 10.9 %copy-start.5 = (f32[64]{0:T(128)S(1)}, f32[64]{0:T(128)}, u32[]{:S(2)}) copy-start(f32[64]{0:T(128)} %param.25) | copy-start | bytes 772
  359.8 62.0 %all-to-all-start.4 = ((bf16[64,12,1024]{2,1,0:T(8,128)(2,1)}), bf16[64,12,1024]{2,1,0:T(8,128)(2,1)}, u32[]{:S(2)}, u32[]{:S(2)}) async-start(bf16[64,12,1024]{2,1,0:T(8,128)(2,1)} %reshape.332), calls=%async_computation.4 | async-start | bytes 4194304 | tf_op jit(solution)/shard_map/all_to_all | solution.py:277
  425.5 11.6 %dynamic-slice-start = ((f32[4096]{0:T(1024)}, s32[]{:T(128)}), f32[1024]{0:T(1024)S(1)}, s32[]{:S(2)}) async-start(f32[4096]{0:T(1024)} %param.23, s32[]{:T(128)} %select_n.33), calls=%async_computation.10 | async-start | bytes 8704 | tf_op jit(solution)/shard_map/dynamic_slice | solution.py:253
Sparse Core Ops, SparseCore 0:
  11.0 84.6 all-gather.11
  123.5 24.6 all-gather.13
  232.6 63.8 all-gather.15
  304.5 45.7 all-gather.17

commit v2 on v1

--- a/solution.py
+++ b/solution.py
@@ -14,6 +14,10 @@
 deep_alpha = 2.0**0.5
 rope_theta = 10000.0
 VMEM_LIMIT = 60 * 1024 * 1024
+MESH = pl.DeviceIdType.MESH
+Z_SIZE = 8
+X_SIZE = 4
+LANES = 4
 
 
 def apply_rotary_heads(block, gain, grid_positions):
@@ -110,76 +114,317 @@
     )(q_t, keys_values, keys_values)
 
 
-def gate_up_kernel(x_ref, wg_ref, wu_ref, h_ref):
-    parts, _, depth = x_ref.shape
-    gate = None
-    up = None
-    for j in range(parts):
-        x = x_ref[j]
-        g = jnp.dot(x, wg_ref[j * depth : (j + 1) * depth, :], preferred_element_type=jnp.float32)
-        u = jnp.dot(x, wu_ref[j * depth : (j + 1) * depth, :], preferred_element_type=jnp.float32)
-        gate = g if gate is None else gate + g
-        up = u if up is None else up + u
-    h_ref[...] = (gate / (1.0 + jnp.exp(-gate)) * up).astype(jnp.bfloat16)
-
-
-def gate_up(x, w_gate, w_up):
-    parts, rows, depth = x.shape
+def half_rows(rows, columns):
+    row = lax.broadcasted_iota(jnp.int32, (rows, columns), 0)
+    return ((row % 8) < 4).astype(jnp.float32)
+
+
+def widened(block, left):
+    value = block.astype(jnp.float32)
+    first = value * left
+    return jnp.concatenate([first, value - first], 1).astype(jnp.bfloat16)
+
+
+def halves_added(value):
+    rows, columns = value.shape
+    parts = value.reshape(rows // 8, 8, columns)
+    return (parts + pltpu.roll(parts, 4, 1)).reshape(rows, columns)
+
+
+def moe_kernel(
+    out_ref,
+    wg_ref,
+    wu_ref,
+    wd_ref,
+    ret_ref,
+    x_ref,
+    h_ref,
+    y_ref,
+    go_send,
+    go_recv,
+    ring_send,
+    ring_recv,
+    pass_send,
+    pass_recv,
+    hid_send,
+    hid_recv,
+    back_send,
+    back_recv,
+):
+    sp = lax.axis_index("sp")
+    lane = lax.axis_index("tp")
+    core = lax.rem(sp, 2)
+    x_at = lax.rem(sp // 2, X_SIZE)
+    z_at = sp // (2 * X_SIZE)
+    right = lax.rem(lane + 1, LANES)
+    left = lax.rem(lane + LANES - 1, LANES)
+    far = lax.rem(lane + 2, LANES)
+    wide = wd_ref.shape[1]
+    half = wide // 2
+    deep = wd_ref.shape[0] // LANES
+    peers = X_SIZE * 2
+    group = 8 * peers
+    count = Z_SIZE
+
+    def z_offset(p):
+        return jnp.where(lax.rem(p, 2) == 1, (p + 1) // 2, lax.rem(Z_SIZE - p // 2, Z_SIZE))
+
+    def peer(index, sign):
+        p = index // peers
+        dx = lax.rem(index, peers) // 2
+        dc = lax.rem(index, 2)
+        z = lax.rem(z_at + sign * z_offset(p) + Z_SIZE, Z_SIZE)
+        x = lax.rem(x_at + sign * dx + X_SIZE, X_SIZE)
+        c = lax.rem(core + dc, 2)
+        return (z * X_SIZE + x) * 2 + c
+
+    def rows_of(index):
+        return pl.ds(pl.multiple_of(index * 8, 8), 8)
+
+    def group_rows(p):
+        return pl.ds(pl.multiple_of(p * group, group), group)
+
+    barrier = pltpu.get_barrier_semaphore()
+
+    def greet(index, _):
+        pl.semaphore_signal(
+            barrier, inc=1, device_id={"sp": peer(index, 1), "tp": lane}, device_id_type=MESH
+        )
+        return 0
+
+    lax.fori_loop(1, count * peers, greet, 0)
+    for other in (left, right, far):
+        pl.semaphore_signal(
+            barrier, inc=1, device_id={"sp": sp, "tp": other}, device_id_type=MESH
+        )
+    pl.semaphore_wait(barrier, count * peers - 1 + LANES - 1)
+
+    def go(index):
+        return pltpu.make_async_remote_copy(
+            src_ref=out_ref.at[rows_of(index)],
+            dst_ref=x_ref.at[lane, rows_of(index)],
+            send_sem=go_send.at[index],
+            recv_sem=go_recv.at[index],
+            device_id={"sp": peer(index, 1), "tp": lane},
+            device_id_type=MESH,
+        )
+
+    def back(index):
+        return pltpu.make_async_remote_copy(
+            src_ref=y_ref.at[rows_of(index)],
+            dst_ref=ret_ref.at[rows_of(index)],
+            send_sem=back_send.at[index],
+            recv_sem=back_recv.at[index],
+            device_id={"sp": peer(index, -1), "tp": lane},
+            device_id_type=MESH,
+        )
+
+    def ring(p, way):
+        return pltpu.make_async_remote_copy(
+            src_ref=x_ref.at[lane, group_rows(p)],
+            dst_ref=x_ref.at[lane, group_rows(p)],
+            send_sem=ring_send.at[p, way],
+            recv_sem=ring_recv.at[p, way],
+            device_id={"sp": sp, "tp": right if way == 0 else left},
+            device_id_type=MESH,
+        )
+
+    def passed(p, way):
+        owner = left if way == 0 else right
+        rows = pl.ds(pl.multiple_of(p * group + way * (group // 2), group // 2), group // 2)
+        return pltpu.make_async_remote_copy(
+            src_ref=x_ref.at[owner, rows],
+            dst_ref=x_ref.at[owner, rows],
+            send_sem=pass_send.at[p, way],
+            recv_sem=pass_recv.at[p, way],
+            device_id={"sp": sp, "tp": right if way == 0 else left},
+            device_id_type=MESH,
+        )
+
+    def hid(p, way):
+        return pltpu.make_async_remote_copy(
+            src_ref=h_ref.at[lane, group_rows(p)],
+            dst_ref=h_ref.at[lane, group_rows(p)],
+            send_sem=hid_send.at[p, way],
+            recv_sem=hid_recv.at[p, way],
+            device_id={"sp": sp, "tp": (right, left, far)[way]},
+            device_id_type=MESH,
+        )
+
+    own_in = pltpu.make_async_copy(
+        out_ref.at[pl.ds(0, 8)], x_ref.at[lane, pl.ds(0, 8)], go_recv.at[0]
+    )
+    own_out = pltpu.make_async_copy(y_ref.at[pl.ds(0, 8)], ret_ref.at[pl.ds(0, 8)], back_recv.at[0])
+    own_in.start()
+
+    def send_one(index, _):
+        go(index).start()
+        return 0
+
+    lax.fori_loop(1, count * peers, send_one, 0)
+
+    def hidden_of(p):
+        rows = group_rows(p)
+        left_half = half_rows(group, half)
+        gate = None
+        up = None
+        for j in range(LANES):
+            lhs = jnp.concatenate(
+                [x_ref[j, rows, :wide], widened(x_ref[j, rows, wide:], left_half)], 0
+            )
+            g = jnp.dot(
+                lhs, wg_ref[j * wide : (j + 1) * wide, :], preferred_element_type=jnp.float32
+            )
+            u = jnp.dot(
+                lhs, wu_ref[j * wide : (j + 1) * wide, :], preferred_element_type=jnp.float32
+            )
+            gate = g if gate is None else gate + g
+            up = u if up is None else up + u
+        gate = jnp.concatenate([gate[:group], halves_added(gate[group:])], 0)
+        up = jnp.concatenate([up[:group], halves_added(up[group:])], 0)
+        hidden = gate / (1.0 + jnp.exp(-gate)) * up
+        low = hidden[group:, : deep // 2]
+        high = hidden[group:, deep // 2 :]
+        narrow = jnp.where(half_rows(group, deep // 2) > 0.0, low, high)
+        h_ref[lane, rows, :deep] = hidden[:group].astype(jnp.bfloat16)
+        h_ref[lane, rows, deep:] = narrow.astype(jnp.bfloat16)
+
+    def output_of(p):
+        rows = group_rows(p)
+        left_half = half_rows(group, deep // 2)
+        total_a = None
+        total_b = None
+        for j in range(LANES):
+            lhs = jnp.concatenate(
+                [h_ref[j, rows, :deep], widened(h_ref[j, rows, deep:], left_half)], 0
+            )
+            z = jnp.dot(
+                lhs, wd_ref[j * deep : (j + 1) * deep, :], preferred_element_type=jnp.float32
+            )
+            a = z[:group].astype(jnp.bfloat16).astype(jnp.float32)
+            b = halves_added(z[group:]).astype(jnp.bfloat16).astype(jnp.float32)
+            total_a = a if total_a is None else total_a + a
+            total_b = b if total_b is None else total_b + b
+        narrow = jnp.where(half_rows(group, half) > 0.0, total_b[:, :half], total_b[:, half:])
+        y_ref[rows, :wide] = total_a.astype(jnp.bfloat16)
+        y_ref[rows, wide:] = narrow.astype(jnp.bfloat16)
+
+    def step(t, _):
+        @pl.when(t < count)
+        def _():
+            @pl.when(t == 0)
+            def _():
+                own_in.wait()
+
+            def arrived(i, _):
+                index = t * peers + i
+
+                @pl.when(index > 0)
+                def _():
+                    go(index).wait_recv()
+
+                return 0
+
+            lax.fori_loop(0, peers, arrived, 0)
+            ring(t, 0).start()
+            ring(t, 1).start()
+
+        @pl.when((t >= 1) & (t < count + 1))
+        def _():
+            ring(t - 1, 0).wait_recv()
+            passed(t - 1, 0).start()
+            ring(t - 1, 1).wait_recv()
+            passed(t - 1, 1).start()
+
+        @pl.when((t >= 2) & (t < count + 2))
+        def _():
+            passed(t - 2, 0).wait_recv()
+            passed(t - 2, 1).wait_recv()
+            hidden_of(t - 2)
+            for way in range(LANES - 1):
+                hid(t - 2, way).start()
+
+        @pl.when(t >= 3)
+        def _():
+            for way in range(LANES - 1):
+                hid(t - 3, way).wait_recv()
+            output_of(t - 3)
+
+            @pl.when(t == 3)
+            def _():
+                own_out.start()
+
+            def send_back(i, _):
+                index = (t - 3) * peers + i
+
+                @pl.when(index > 0)
+                def _():
+                    back(index).start()
+
+                return 0
+
+            lax.fori_loop(0, peers, send_back, 0)
+
+        return 0
+
+    lax.fori_loop(0, count + 3, step, 0)
+    own_out.wait()
+
+    def finish(index, _):
+        go(index).wait_send()
+        back(index).wait_send()
+        back(index).wait_recv()
+        return 0
+
+    lax.fori_loop(1, count * peers, finish, 0)
+
+    def finish_group(p, _):
+        for way in range(2):
+            ring(p, way).wait_send()
+            passed(p, way).wait_send()
+        for way in range(LANES - 1):
+            hid(p, way).wait_send()
+        return 0
+
+    lax.fori_loop(0, count, finish_group, 0)
+
+
+def moe_layer(outgoing, w_gate, w_up, w_down):
+    rows, columns = outgoing.shape
     hidden = w_gate.shape[1]
-    block = rows // 4
+    blocks = rows // 8
+    vmem = pl.BlockSpec(memory_space=pltpu.VMEM)
+    dma = pltpu.SemaphoreType.DMA
     return pl.pallas_call(
-        gate_up_kernel,
-        grid=(rows // block,),
-        in_specs=[
-            pl.BlockSpec((parts, block, depth), lambda i: (0, i, 0)),
-            pl.BlockSpec(w_gate.shape, lambda i: (0, 0)),
-            pl.BlockSpec(w_up.shape, lambda i: (0, 0)),
+        moe_kernel,
+        in_specs=[vmem] * 4,
+        out_specs=vmem,
+        out_shape=jax.ShapeDtypeStruct((rows, columns), jnp.bfloat16),
+        scratch_shapes=[
+            pltpu.VMEM((LANES, rows, columns), jnp.bfloat16),
+            pltpu.VMEM((LANES, rows, hidden * 3 // 2), jnp.bfloat16),
+            pltpu.VMEM((rows, columns), jnp.bfloat16),
+            dma((blocks,)),
+            dma((blocks,)),
+            dma((Z_SIZE, 2)),
+            dma((Z_SIZE, 2)),
+            dma((Z_SIZE, 2)),
+            dma((Z_SIZE, 2)),
+            dma((Z_SIZE, LANES - 1)),
+            dma((Z_SIZE, LANES - 1)),
+            dma((blocks,)),
+            dma((blocks,)),
         ],
-        out_specs=pl.BlockSpec((block, hidden), lambda i: (i, 0)),
-        out_shape=jax.ShapeDtypeStruct((rows, hidden), jnp.bfloat16),
-        compiler_params=pltpu.CompilerParams(vmem_limit_bytes=VMEM_LIMIT),
+        compiler_params=pltpu.CompilerParams(
+            vmem_limit_bytes=VMEM_LIMIT, collective_id=1, has_side_effects=True
+        ),
         cost_estimate=pl.CostEstimate(
-            flops=4 * rows * parts * depth * hidden,
-            bytes_accessed=2 * parts * depth * (rows + 2 * hidden),
-            transcendentals=rows * hidden,
-        ),
-        name="gate_up",
-    )(x, w_gate, w_up)
-
-
-def down_kernel(h_ref, w_ref, o_ref):
-    parts, _, depth = h_ref.shape
-    total = None
-    for j in range(parts):
-        part = jnp.dot(
-            h_ref[j], w_ref[j * depth : (j + 1) * depth, :], preferred_element_type=jnp.float32
-        )
-        part = part.astype(jnp.bfloat16).astype(jnp.float32)
-        total = part if total is None else total + part
-    o_ref[...] = total.astype(jnp.bfloat16)
-
-
-def down(h, w):
-    parts, rows, depth = h.shape
-    width = w.shape[1]
-    block = rows // 4
-    return pl.pallas_call(
-        down_kernel,
-        grid=(rows // block,),
-        in_specs=[
-            pl.BlockSpec((parts, block, depth), lambda i: (0, i, 0)),
-            pl.BlockSpec(w.shape, lambda i: (0, 0)),
-        ],
-        out_specs=pl.BlockSpec((block, width), lambda i: (i, 0)),
-        out_shape=jax.ShapeDtypeStruct((rows, width), jnp.bfloat16),
-        compiler_params=pltpu.CompilerParams(vmem_limit_bytes=VMEM_LIMIT),
-        cost_estimate=pl.CostEstimate(
-            flops=2 * rows * parts * depth * width,
-            bytes_accessed=2 * parts * depth * (rows + width) + 2 * rows * width,
+            flops=12 * LANES * rows * 1024 * hidden,
+            bytes_accessed=200_000_000,
             transcendentals=0,
         ),
-        name="down",
-    )(h, w)
+        name="experts",
+    )(outgoing, w_gate, w_up, w_down)
 
 
 def split_layer_norm(z, gain):
@@ -254,42 +499,56 @@
     x_one = split_layer_norm(summed, gain_one).astype(jnp.bfloat16)
 
     top = ids.shape[1]
-    per_expert = lanes * CAP
+    half = part // 2
     blocks = ids.reshape(lanes, own * top)
     one_hot = (blocks[:, :, None] == jnp.arange(sp_count, dtype=jnp.int32)).astype(jnp.int32)
     earlier = jnp.cumsum(one_hot, 1) - one_hot
     rank = jnp.sum(earlier * one_hot, 2)
-    slot = blocks * per_expert + jnp.arange(lanes, dtype=jnp.int32)[:, None] * CAP + rank
-    slot = slot.reshape(tokens, top)
-    slots = sp_count * per_expert
-    chosen = slot[:, :, None] == jnp.arange(slots, dtype=jnp.int32)
-    placing = jnp.any(chosen, 1).astype(jnp.bfloat16)
-    outgoing = lax.dot_general(
-        placing, x_one, (((0,), (0,)), ((), ())), preferred_element_type=jnp.float32
+    sp = lax.axis_index("sp")
+    dz = (blocks // (2 * X_SIZE) - sp // (2 * X_SIZE)) % Z_SIZE
+    dx = (blocks // 2 - sp // 2) % X_SIZE
+    dc = (blocks - sp) % 2
+    near = jnp.where(dz == 0, 0, jnp.where(dz <= Z_SIZE // 2, 2 * dz - 1, 2 * (Z_SIZE - dz)))
+    target = (near * X_SIZE + dx) * 2 + dc
+    place = jnp.arange(lanes, dtype=jnp.int32)[:, None] * CAP + rank
+    row_a = jnp.where(place < 8, target * 8 + place, -1).reshape(tokens, top)
+    row_b = jnp.where(place < 8, -1, target * 8 + place - 8).reshape(tokens, top)
+    rows = jnp.arange(sp_count * 8, dtype=jnp.int32)
+    picks = (row_a[:, :, None] == rows, row_b[:, :, None] == rows, row_b[:, :, None] + 4 == rows)
+    picks = (picks[0], picks[1] & (row_b[:, :, None] >= 0), picks[2] & (row_b[:, :, None] >= 0))
+
+    def placed(pick, source):
+        return lax.dot_general(
+            jnp.any(pick, 1).astype(jnp.bfloat16),
+            source,
+            (((0,), (0,)), ((), ())),
+            preferred_element_type=jnp.float32,
+        )
+
+    outgoing = jnp.concatenate(
+        [
+            placed(picks[0], x_one),
+            placed(picks[1], x_one[:, :half]) + placed(picks[2], x_one[:, half:]),
+        ],
+        1,
     ).astype(jnp.bfloat16)
-    received = lax.all_to_all(
-        outgoing.reshape(sp_count, per_expert, part), "sp", split_axis=0, concat_axis=0, tiled=True
+    returned = moe_layer(outgoing, gate_proj[0], up_proj[0], down_slice)
+
+    def weighted(pick, source):
+        weights = jnp.sum(jnp.where(pick, gates[:, :, None], 0.0), 1)
+        total = None
+        for _ in range(3):
+            term = lax.reduce_precision(weights, 8, 7)
+            weights = weights - term
+            piece = jnp.dot(
+                term.astype(jnp.bfloat16), source, preferred_element_type=jnp.float32
+            )
+            total = piece if total is None else total + piece
+        return total
+
+    moe = weighted(picks[0], returned[:, :part]) + jnp.concatenate(
+        [weighted(picks[1], returned[:, part:]), weighted(picks[2], returned[:, part:])], 1
     )
-    gathered = lax.all_gather(received.reshape(slots, part), "tp", axis=0, tiled=False)
-    hidden = gate_up(gathered, gate_proj[0], up_proj[0])
-    hidden = lax.all_gather(hidden, "tp", axis=0, tiled=False)
-    expert_out = down(hidden, down_slice)
-    returned = lax.all_to_all(
-        expert_out.reshape(sp_count, per_expert, part),
-        "sp",
-        split_axis=0,
-        concat_axis=0,
-        tiled=True,
-    ).reshape(slots, part)
-    weights = jnp.sum(jnp.where(chosen, gates[:, :, None], 0.0), 1)
-    moe = None
-    for _ in range(3):
-        term = lax.reduce_precision(weights, 8, 7)
-        weights = weights - term
-        piece = jnp.dot(
-            term.astype(jnp.bfloat16), returned, preferred_element_type=jnp.float32
-        )
-        moe = piece if moe is None else moe + piece
     final = deep_alpha * x_one.astype(jnp.float32) + moe
     mixed = split_layer_norm(final, gain_two).astype(jnp.bfloat16)
     return lax.all_to_all(mixed, "tp", split_axis=0, concat_axis=1, tiled=True)

time: 458 us -> 330 us (0.72)
  waiting for transfers between devices: 176 us -> 50.9 us
  Pallas kernels: 41.1 us -> 146 us
  blocking collectives: 154 us -> 60.6 us
  local copies, waits for them, and re-layouts: 33.7 us -> 22.3 us
  starting transfers between devices: 20.7 us -> 14 us
    pallas_call x2 -> x1, Pallas kernels: 13.5 us -> 118 us  [moe_layer(): pl.pallas_call(moe_kernel, in_specs=[vmem] * 4, out_specs=vmem, out_shape...]
    all_to_all x2 -> x0, blocking collectives: 104 us -> none  [the longest x1 61.7 us: per_device(): lax.all_to_all(outgoing.reshape(sp_count, per_expert, part), 'sp', split_...]
    all_gather x2 -> x0, waiting for transfers between devices: 63.7 us -> none  [the longest x1 63.7 us: per_device(): lax.all_gather(received.reshape(slots, part), 'tp', axis=0, tiled=False)]
    all_to_all x1, waiting for transfers between devices: 42.6 us -> 0.01 us  [per_device(): lax.all_to_all(down_proj[0], 'tp', split_axis=1, concat_axis=0, tiled=True)]
    all_gather x1, waiting for transfers between devices: 61.1 us -> 45.5 us  [per_device(): keys_values = lax.all_gather(both, 'sp', axis=0, tiled=True)]
    reshape x3 -> x0, local copies, waits for them, and re-layouts: 8.46 us -> none  [the longest x1 3.6 us: per_device(): expert_out.reshape(sp_count, per_expert, part)]
    all_gather x2, blocking collectives: 20.9 us -> 28 us  [split_layer_norm(): both = lax.all_gather(jnp.stack([mean, m2]), 'tp', axis=0, tiled=False)]
    all_to_all x1, starting transfers between devices: 10.9 us -> 4.46 us  [per_device(): lax.all_to_all(down_proj[0], 'tp', split_axis=1, concat_axis=0, tiled=True)]
  transfers between devices with their start and end apart: 7 -> 5, of which waited for: 5 -> 2; matrix products, arithmetic and copies ran while one was open for 5% -> 9% of each run, Pallas kernels for 6% -> 8%
where the time goes in v2:
time: 330 us; the launch traced here: 329 us
  Pallas kernels  146 us (44%)
  blocking collectives  60.6 us (18%)
  waiting for transfers between devices  50.9 us (15%)
  local copies, waits for them, and re-layouts  22.3 us (7%)
  starting transfers between devices  14 us (4%)
  between operations  13.9 us (4%)
  other arithmetic  11.4 us (3%)
  matrix products  9.75 us (3%)
    pallas_call x1, Pallas kernels, moe_layer(): pl.pallas_call(moe_kernel, in_specs=[vmem] * 4, out_specs=vmem, out_shape...  118 us
    all_gather x1, waiting for transfers between devices, per_device(): keys_values = lax.all_gather(both, 'sp', axis=0, tiled=True)  45.5 us
    all_gather x2, blocking collectives, split_layer_norm(): both = lax.all_gather(jnp.stack([mean, m2]), 'tp', axis=0, tiled=False)  28 us
    pallas_call x1, Pallas kernels, attention(): pl.pallas_call(attention_kernel, grid=(length // block,), in_specs=[pl.Bl...  27.7 us
    all_to_all x1, blocking collectives, per_device(): return lax.all_to_all(mixed, 'tp', split_axis=0, concat_axis=1, tiled=True)  11.6 us
    all_gather x1, blocking collectives, per_device(): ids = lax.all_gather(expert_ids, 'tp', axis=0, tiled=True)  11.3 us
    all_gather x1, blocking collectives, per_device(): gates = lax.all_gather(gates_own, 'tp', axis=0, tiled=True)  9.72 us
    unnamed x18, local copies, waits for them, and re-layouts  7.58 us
  transfers between devices with their start and end apart: 5, of which 2 were waited for; matrix products, arithmetic and copies ran while one was open for 9% of the time, Pallas kernels for 8%

profile of v2, /device:TPU:2, one launch (start us, length us, event | category | flops | bytes accessed | tf_op | source)
XLA Modules:
  0.0 328.6 jit_solution(15659820646678841228)
XLA Ops:
  6.6 1.0 fusion.35
  7.6 0.9 fusion.37
  8.7 0.6 fusion.38
  9.3 1.6 pad_maximum_fusion.4
  10.9 0.8 copy.127
  11.7 4.6 %all-to-all-start = ((bf16[64,4,1024]{2,0,1:T(8,128)(2,1)}), bf16[64,4,1024]{2,0,1:T(8,128)(2,1)S(1)}, u32[]{:S(2)}, u32[]{:S(2)}) async-start(bf16[64,4,1024]{2,0,1:T(8,128)(2,1)} %bitcast.66), calls=%async_computation | async-start | bytes 1048576 | tf_op jit(solution)/shard_map/all_to_all | solution.py:477
  16.5 0.3 multiply_reduce_fusion.2
  16.9 0.3 multiply_multiply_fusion
  17.3 11.3 %all-gather.3 = s32[4,64,2]{1,2,0:T(2,128)S(1)} all-gather(s32[1,64,2]{1,2,0:T(2,128)S(1)} %bitcast.80), channel_id=1, replica_groups=mesh['sp'=64,'tp'=4] {'tp'}, dimensions={0}, use_global_device_ids=true | all-gather | bytes 2560 | tf_op jit(solution)/shard_map/all_gather | solution.py:478
  28.7 6.5 %copy.105 = bf16[512,4096]{0,1:T(8,128)(2,1)} copy(bf16[512,4096]{1,0:T(8,128)(2,1)} %param.21) | data formatting | bytes 8388608 | tf_op args[6]
  35.2 0.5 fusion.43
  35.7 0.5 subtract_convert_fusion
  36.3 4.9 %all-to-all-start.1 = ((bf16[512,4,1024]{0,2,1:T(8,128)(2,1)}), bf16[512,4,1024]{0,2,1:T(8,128)(2,1)}, u32[]{:S(2)}, u32[]{:S(2)}) async-start(bf16[512,4,1024]{0,2,1:T(8,128)(2,1)} %bitcast.67), calls=%async_computation.1 | async-start | bytes 8388608 | tf_op jit(solution)/shard_map/all_to_all | solution.py:475
  41.3 0.5 reduce-precision_convert_fusion.6
  41.8 0.3 maximum_bitcast_fusion
  42.0 0.6 copy.104
  42.7 0.9 copy.122
  43.8 0.3 reduce_window_sum.11
  44.8 3.3 %all_to_all.58 = bf16[256,4,1024]{2,1,0:T(4,128)(2,1)S(1)} reshape(bf16[1,256,4096]{2,1,0:T(8,128)(2,1)} %param.29) | data formatting | bytes 4194304 | tf_op jit(solution)/shard_map/all_to_all | solution.py:476
  48.1 2.0 copy.114
  50.1 45.5 %all-gather.9.cloned.1.call-done.k_ref.v_ref = bf16[16384,256]{1,0:T(8,128)(2,1)} async-done(((bf16[256,256]{1,0:T(8,128)(2,1)}), bf16[16384,256]{1,0:T(8,128)(2,1)}) %all-gather.9.cloned.1.call-update) | async-done | bytes 8388624 | tf_op jit(solution)/shard_map/all_gather | solution.py:473
  95.7 27.7 %attention.1 = bf16[256,512]{1,0:T(8,128)(2,1)} custom-call(bf16[256,1024]{1,0:T(8,128)(2,1)} %bitcast.74, bf16[16384,256]{1,0:T(8,128)(2,1)} %all-gather.9.cloned.1.call-done.k_ref.v_ref, bf16[16384,256]{1,0:T(8,128)(2,1)} %all-gather.9.cloned.1.call-done.k_ref.v_ref), custom_call_target="tpu_custom_call" | custom-call | flops 8589934592 | bytes 8388608 | tf_op jit(solution)/shard_map/attention/pallas_call | solution.py:92
  123.4 9.7 %all-gather.4 = f32[4,64,2]{1,2,0:T(2,128)S(1)} all-gather(f32[1,64,2]{1,2,0:T(2,128)S(1)} %divide_bitcast_fusion), channel_id=1, replica_groups=mesh['sp'=64,'tp'=4] {'tp'}, dimensions={0}, use_global_device_ids=true | all-gather | bytes 2560 | tf_op jit(solution)/shard_map/all_gather | solution.py:482
  133.5 0.4 fusion.8
  133.9 0.9 select_reduce_fusion.1
  134.9 4.5 %all-to-all-start.2 = ((bf16[256,4,1024]{2,0,1:T(8,128)(2,1)}), bf16[256,4,1024]{2,0,1:T(8,128)(2,1)}, u32[]{:S(2)}, u32[]{:S(2)}) async-start(bf16[256,4,1024]{2,0,1:T(8,128)(2,1)} %copy.114), calls=%async_computation.2 | async-start | bytes 4194304 | tf_op jit(solution)/shard_map/all_to_all | solution.py:476
  139.4 6.3 %copy.106 = bf16[4,512,1024]{2,1,0:T(8,128)(2,1)} copy(bf16[4,512,1024]{1,2,0:T(8,128)(2,1)} %bitcast.9) | data formatting | bytes 8388608 | tf_op jit(solution)/shard_map/all_to_all | solution.py:475
  145.7 5.3 %all-gather.11.cloned.1.call-done = bf16[256,2048]{1,0:T(8,128)(2,1)} async-done(((bf16[256,512]{1,0:T(8,128)(2,1)}), bf16[256,2048]{1,0:T(8,128)(2,1)}) %all-gather.11.cloned.1.call-update) | async-done | bytes 1048592 | tf_op jit(solution)/shard_map/all_gather | solution.py:492
  151.0 3.9 %fusion.59 = (f32[256]{0:T(256)S(1)}, f32[256,1024]{1,0:T(8,128)S(1)}) fusion(f32[256,1024]{1,0:T(8,128)S(1)} %bitcast.72, bf16[256,2048]{1,0:T(8,128)(2,1)} %all-gather.11.cloned.1.call-done, bf16[2048,1024]{1,0:T(8,128)(2,1)} %bitcast.68), kind=kOutput, calls=%fused_computation.160 | convolution fusion | flops 1074528000 | bytes 7341056 | tf_op jit(solution)/shard_map/dot_general | solution.py:494
  155.1 17.6 %all-gather.2 = f32[4,2,256]{2,1,0:T(2,128)S(1)} all-gather(f32[1,2,256]{2,1,0:T(2,128)S(1)} %maximum_bitcast_fusion.1), channel_id=2, replica_groups=mesh['sp'=64,'tp'=4] {'tp'}, dimensions={0}, use_global_device_ids=true | all-gather | bytes 10240 | tf_op jit(solution)/shard_map/all_gather | solution.py:435
  173.0 0.3 fusion.26
  173.4 0.5 convolution_convert_fusion
  173.9 0.3 fusion.3
  174.2 1.3 pad_maximum_fusion.out_ref
  175.5 118.0 %experts.1 = bf16[512,1536]{1,0:T(8,128)(2,1)} custom-call(bf16[512,1536]{1,0:T(8,128)(2,1)} %pad_maximum_fusion.out_ref, bf16[4096,256]{1,0:T(8,128)(2,1)} %bitcast.81, bf16[4096,256]{1,0:T(8,128)(2,1)} %bitcast.82, bf16[1024,1024]{1,0:T(8,128)(2,1)} %bitcast.20.wd_ref), custom_call_target="tpu_custom_call" | custom-call | flops 6442450944 | bytes 200000000 | tf_op jit(solution)/shard_map/experts/pallas_call | solution.py:398
  293.5 1.8 fusion.11
  295.3 0.4 convolution_add_fusion.1
  295.8 0.3 fusion.23
  296.1 0.3 convolution_add_fusion.6
  296.4 0.3 convolution_add_fusion.5
  296.7 0.3 fusion.24
  297.0 0.3 convolution_add_fusion.4
  297.4 0.3 convolution_add_fusion.3
  297.7 0.6 fusion.60
  298.3 0.3 multiply_reduce_fusion
  298.6 10.4 %all-gather.5 = f32[4,2,256]{2,1,0:T(2,128)S(1)} all-gather(f32[1,2,256]{2,1,0:T(2,128)S(1)} %maximum_bitcast_fusion.2), channel_id=3, replica_groups=mesh['sp'=64,'tp'=4] {'tp'}, dimensions={0}, use_global_device_ids=true | all-gather | bytes 10240 | tf_op jit(solution)/shard_map/all_gather | solution.py:435
  309.3 11.6 %all_to_all.70 = bf16[4,64,1024]{2,1,0:T(8,128)(2,1)S(1)} all-to-all(bf16[4,64,1024]{2,1,0:T(8,128)(2,1)S(1)} %bitcast.69), channel_id=1, replica_groups=mesh['sp'=64,'tp'=4] {'tp'}, dimensions={0} | all-to-all | bytes 1048576 | tf_op jit(solution)/shard_map/all_to_all | solution.py:554
  320.9 0.8 copy.121
  (66 shorter events, 2.8 us)
Async XLA Ops:
  6.5 4.4 %copy-start.1 = (bf16[64,4096]{1,0:T(8,128)(2,1)S(1)}, bf16[64,4096]{1,0:T(8,128)(2,1)}, u32[]{:S(2)}) copy-start(bf16[64,4096]{1,0:T(8,128)(2,1)} %param.15) | copy-start | bytes 1572868
  6.5 89.2 %all-gather.9.cloned.1.call-start = ((), (), s32[]{:S(2)}) async-start(), calls=%async_computation.4 | async-start | bytes 8519680 | tf_op jit(solution)/shard_map/all_gather | solution.py:473
  8.7 7.7 %copy-start.2 = (bf16[256,512]{1,0:T(8,128)(2,1)S(1)}, bf16[256,512]{1,0:T(8,128)(2,1)}, u32[]{:S(2)}) copy-start(bf16[256,512]{1,0:T(8,128)(2,1)} %param.16) | copy-start | bytes 786436
  11.7 5.2 %copy-start.5 = (f32[128]{0:T(128)S(1)}, f32[128]{0:T(128)}, u32[]{:S(2)}) copy-start(f32[128]{0:T(128)} %param.19) | copy-start | bytes 1540
  11.7 24.5 %all-to-all-start = ((bf16[64,4,1024]{2,0,1:T(8,128)(2,1)}), bf16[64,4,1024]{2,0,1:T(8,128)(2,1)S(1)}, u32[]{:S(2)}, u32[]{:S(2)}) async-start(bf16[64,4,1024]{2,0,1:T(8,128)(2,1)} %bitcast.66), calls=%async_computation | async-start | bytes 1048576 | tf_op jit(solution)/shard_map/all_to_all | solution.py:477
  16.3 0.9 copy-start.4
  36.3 98.6 %all-to-all-start.1 = ((bf16[512,4,1024]{0,2,1:T(8,128)(2,1)}), bf16[512,4,1024]{0,2,1:T(8,128)(2,1)}, u32[]{:S(2)}, u32[]{:S(2)}) async-start(bf16[512,4,1024]{0,2,1:T(8,128)(2,1)} %bitcast.67), calls=%async_computation.1 | async-start | bytes 8388608 | tf_op jit(solution)/shard_map/all_to_all | solution.py:475
  41.2 109.8 %all-gather.11.cloned.1.call-start = ((), (), s32[]{:S(2)}) async-start(), calls=%async_computation.5 | async-start | bytes 1310720 | tf_op jit(solution)/shard_map/all_gather | solution.py:492
  48.1 2.0 copy-start.3
  95.7 27.7 %copy-start.6 = (f32[64]{0:T(128)S(1)}, f32[64]{0:T(128)}, u32[]{:S(2)}) copy-start(f32[64]{0:T(128)} %param.25) | copy-start | bytes 772
  134.9 40.6 %all-to-all-start.2 = ((bf16[256,4,1024]{2,0,1:T(8,128)(2,1)}), bf16[256,4,1024]{2,0,1:T(8,128)(2,1)}, u32[]{:S(2)}, u32[]{:S(2)}) async-start(bf16[256,4,1024]{2,0,1:T(8,128)(2,1)} %copy.114), calls=%async_computation.2 | async-start | bytes 4194304 | tf_op jit(solution)/shard_map/all_to_all | solution.py:476
  151.0 21.8 %dynamic-slice-start.1 = ((f32[4096]{0:T(1024)}, s32[]{:T(128)}), f32[1024]{0:T(1024)S(1)}, s32[]{:S(2)}) async-start(f32[4096]{0:T(1024)} %param.22, s32[]{:T(128)} %select_n.123), calls=%async_computation.7 | async-start | bytes 8704 | tf_op jit(solution)/shard_map/dynamic_slice | solution.py:497
  293.5 1.8 copy-start
  297.7 11.4 %dynamic-slice-start = ((f32[4096]{0:T(1024)}, s32[]{:T(128)}), f32[1024]{0:T(1024)S(1)}, s32[]{:S(2)}) async-start(f32[4096]{0:T(1024)} %param.23, s32[]{:T(128)} %select_n.123), calls=%async_computation.6 | async-start | bytes 8704 | tf_op jit(solution)/shard_map/dynamic_slice | solution.py:498
Sparse Core Ops, SparseCore 0:
  11.0 84.6 all-gather.8
  123.5 27.4 all-gather.10

commit v3 on v2

--- a/solution.py
+++ b/solution.py
@@ -8,7 +8,6 @@
 
 GRID_W = 64
 CAP = 3
-KEY_BLOCK = 1024
 QUERY_TILE = 512
 
 deep_alpha = 2.0**0.5
@@ -38,80 +37,460 @@
     return turned.astype(jnp.bfloat16)
 
 
-def attention_kernel(qt_ref, k_ref, v_ref, o_ref, m_ref, l_ref, acc_ref):
-    step = pl.program_id(0)
+def front_kernel(
+    qt_ref,
+    own_ref,
+    w_ref,
+    wd_ref,
+    resid_ref,
+    info_ref,
+    gain_ref,
+    x_ref,
+    down_ref,
+    table_ref,
+    kv_ref,
+    m_ref,
+    l_ref,
+    acc_ref,
+    attn_ref,
+    out_ref,
+    res_ref,
+    stat_ref,
+    tx,
+    rx_full,
+    rx_half,
+    rx_core,
+    load_sem,
+    w_send,
+    w_recv,
+    w_pair_send,
+    w_pair_recv,
+    d_send,
+    d_recv,
+    r_send,
+    r_recv,
+    i_send,
+    i_recv,
+    a_send,
+    a_recv,
+    s_send,
+    s_recv,
+):
+    sp = lax.axis_index("sp")
+    lane = lax.axis_index("tp")
+    core = lax.rem(sp, 2)
+    x_at = lax.rem(sp // 2, X_SIZE)
+    z_at = sp // (2 * X_SIZE)
+    partner = sp + 1 - 2 * core
+    block = own_ref.shape[0]
+    width = own_ref.shape[1] // 2
     rows = qt_ref.shape[1]
-    width = v_ref.shape[1]
-    heads = o_ref.shape[1] // width
-    tokens = o_ref.shape[0]
-
-    @pl.when(step == 0)
-    def _():
-        m_ref[...] = jnp.full_like(m_ref, -1e30)
-        l_ref[...] = jnp.zeros_like(l_ref)
-        acc_ref[...] = jnp.zeros_like(acc_ref)
-
-    k = k_ref[...]
-    k_twice = jnp.concatenate([k, k], 1)
-    v_t = v_ref[...].T
+    heads = rows // block
+    wide = x_ref.shape[1]
+    lane_rows = res_ref.shape[1]
+    depth = out_ref.shape[1]
+    lanes_of = [lax.rem(lane + 1, LANES), lax.rem(lane + LANES - 1, LANES), lax.rem(lane + 2, LANES)]
+    froms = [lanes_of[1], lanes_of[0], lanes_of[2]]
+
+    def sp_of(z, x, c):
+        return (lax.rem(z + 2 * Z_SIZE, Z_SIZE) * X_SIZE + lax.rem(x + 2 * X_SIZE, X_SIZE)) * 2 + c
+
+    ways = (
+        sp_of(z_at + 1, x_at, core),
+        sp_of(z_at - 1, x_at, core),
+        sp_of(z_at, x_at + 1, core),
+        sp_of(z_at, x_at - 1, core),
+        partner,
+    )
+    barrier = pltpu.get_barrier_semaphore()
+    for way in range(5):
+        pl.semaphore_signal(
+            barrier, inc=1, device_id={"sp": ways[way], "tp": lane}, device_id_type=MESH
+        )
+    for other in lanes_of:
+        pl.semaphore_signal(
+            barrier, inc=1, device_id={"sp": sp, "tp": other}, device_id_type=MESH
+        )
+
+    own_copy = pltpu.make_async_copy(own_ref, kv_ref.at[core, z_at, x_at], load_sem.at[0])
+    w_copy = pltpu.make_async_copy(
+        w_ref.at[:, pl.ds(pl.multiple_of(lane * wide, wide), wide)], out_ref.at[lane], load_sem.at[1]
+    )
+    d_copy = pltpu.make_async_copy(
+        wd_ref.at[:, pl.ds(pl.multiple_of(lane * wide, wide), wide)], down_ref.at[lane], load_sem.at[2]
+    )
+    r_copy = pltpu.make_async_copy(
+        resid_ref.at[:, pl.ds(pl.multiple_of(lane * wide, wide), wide)], res_ref.at[lane], load_sem.at[3]
+    )
+    i_copy = pltpu.make_async_copy(info_ref, table_ref.at[lane], load_sem.at[4])
+    own_copy.start()
+
+    def to_lane(src, dst, send, recv, way):
+        return pltpu.make_async_remote_copy(
+            src_ref=src,
+            dst_ref=dst,
+            send_sem=send.at[way],
+            recv_sem=recv.at[way],
+            device_id={"sp": sp, "tp": lanes_of[way]},
+            device_id_type=MESH,
+        )
+
+    def columns(way):
+        return pl.ds(pl.multiple_of(lanes_of[way] * wide, wide), wide)
+
+    part_rows = depth // 2
+    half = pl.ds(pl.multiple_of(core * part_rows, part_rows), part_rows)
+
+    def w_go(way):
+        return to_lane(w_ref.at[half, columns(way)], out_ref.at[lane, half], w_send, w_recv, way)
+
+    def w_pair(way):
+        return pltpu.make_async_remote_copy(
+            src_ref=out_ref.at[froms[way], half],
+            dst_ref=out_ref.at[froms[way], half],
+            send_sem=w_pair_send.at[way],
+            recv_sem=w_pair_recv.at[way],
+            device_id={"sp": partner, "tp": lane},
+            device_id_type=MESH,
+        )
+
+    def d_go(way):
+        return to_lane(wd_ref.at[:, columns(way)], down_ref.at[lane], d_send, d_recv, way)
+
+    def r_go(way):
+        return to_lane(resid_ref.at[:, columns(way)], res_ref.at[lane], r_send, r_recv, way)
+
+    def i_go(way):
+        return to_lane(info_ref, table_ref.at[lane], i_send, i_recv, way)
+
+    def a_go(way):
+        return to_lane(attn_ref.at[lane], attn_ref.at[lane], a_send, a_recv, way)
+
+    def s_go(way):
+        return to_lane(stat_ref.at[lane], stat_ref.at[lane], s_send, s_recv, way)
+
+    def send(cls, zz, xx, way, piece=None):
+        if piece is None:
+            at = kv_ref.at[cls, zz, xx]
+            recv = rx_core.at[zz, xx] if way == 4 else rx_full.at[zz, xx]
+        else:
+            at = kv_ref.at[cls, zz, xx, pl.ds(piece * (block // 2), block // 2)]
+            recv = rx_half.at[zz, xx, piece]
+        return pltpu.make_async_remote_copy(
+            src_ref=at,
+            dst_ref=at,
+            send_sem=tx.at[zz, xx, way],
+            recv_sem=recv,
+            device_id={"sp": ways[way], "tp": lane},
+            device_id_type=MESH,
+        )
+
+    def wait_block(zz, xx, halves):
+        if halves:
+            send(core, zz, xx, 0, 0).wait_recv()
+            send(core, zz, xx, 0, 1).wait_recv()
+        else:
+            send(core, zz, xx, 0).wait_recv()
+
+    def z_of(d):
+        return lax.rem(z_at + d + Z_SIZE, Z_SIZE)
+
+    x_order = [
+        x_at,
+        lax.rem(x_at + X_SIZE - 1, X_SIZE),
+        lax.rem(x_at + 1, X_SIZE),
+        lax.rem(x_at + 2, X_SIZE),
+    ]
+
+    def along_x(zz, s, act):
+        if s == 0:
+            act(send(core, zz, x_order[0], 2))
+            act(send(core, zz, x_order[0], 3))
+        elif s == 1:
+            act(send(core, zz, x_order[1], 2, 0))
+        elif s == 2:
+            act(send(core, zz, x_order[2], 3, 1))
+
+    def along_z(h, xx, side, act):
+        zz = z_of(-h if side == 0 else h)
+
+        @pl.when(h < 3)
+        def _():
+            act(send(core, zz, xx, side))
+
+        @pl.when(h == 3)
+        def _():
+            act(send(core, zz, xx, side, side))
+
+    def first(s, act, wait):
+        xx = x_order[s]
+        if wait and s > 0:
+            wait_block(z_at, xx, s == 3)
+        along_x(z_at, s, act)
+
+        if s == 0:
+            act(send(core, z_at, xx, 0))
+            act(send(core, z_at, xx, 1))
+        else:
+
+            @pl.when(core == 0)
+            def _():
+                act(send(core, z_at, xx, 0))
+                act(send(core, z_at, xx, 1))
+
+        act(send(core, z_at, xx, 4))
+
+    def later(h, s, act, wait):
+        xx = x_order[s]
+
+        @pl.when(h < 4)
+        def _():
+            for side in range(2):
+                zz = z_of(-h if side == 0 else h)
+
+                @pl.when(core == 0)
+                def _():
+                    if wait:
+                        wait_block(zz, xx, False)
+                    along_z(h, xx, side, act)
+
+                @pl.when(core == 1)
+                def _():
+                    if wait:
+                        wait_block(zz, xx, s == 3)
+                    if s == 0:
+                        along_z(h, xx, side, act)
+                    along_x(zz, s, act)
+
+                act(send(core, zz, xx, 4))
+
+        @pl.when(h == 4)
+        def _():
+            zz = z_of(4)
+            if wait:
+                if s in (0, 3):
+                    wait_block(zz, xx, True)
+                else:
+
+                    @pl.when(core == 0)
+                    def _():
+                        wait_block(zz, xx, True)
+
+                    @pl.when(core == 1)
+                    def _():
+                        wait_block(zz, xx, False)
+
+            @pl.when(core == 1)
+            def _():
+                along_x(zz, s, act)
+
+            act(send(core, zz, xx, 4))
+
+    def start(copy):
+        copy.start()
+
+    def ended(copy):
+        copy.wait_send()
+
+    m_ref[...] = jnp.full_like(m_ref, -1e30)
+    l_ref[...] = jnp.zeros_like(l_ref)
+    acc_ref[...] = jnp.zeros_like(acc_ref)
+    own_copy.wait()
+    pl.semaphore_wait(barrier, 5 + LANES - 1)
+    first(0, start, True)
+    for way in range(LANES - 1):
+        i_go(way).start()
+    for way in range(LANES - 1):
+        w_go(way).start()
+    for way in range(LANES - 1):
+        r_go(way).start()
+    for way in range(2):
+        d_go(way).start()
+    w_copy.start()
+    r_copy.start()
+    d_copy.start()
+    i_copy.start()
+    for s in range(1, 4):
+        first(s, start, True)
+
     tile = min(QUERY_TILE, rows)
-    count = rows // tile
-
-    def scores(t):
-        return jnp.dot(
-            k_twice, qt_ref[:, t * tile : (t + 1) * tile], preferred_element_type=jnp.float32
-        )
-
-    s = scores(0)
-    for t in range(count):
-        following = scores(t + 1) if t + 1 < count else None
-        at = slice(t * tile, (t + 1) * tile)
-        m_old = m_ref[:, at]
-        m_new = jnp.maximum(m_old, jnp.max(s, 0, keepdims=True))
-        shrink = jnp.exp2(m_old - m_new)
-        p = jnp.exp2(s - m_new)
-        l_ref[:, at] = l_ref[:, at] * shrink + jnp.sum(p, 0, keepdims=True)
-        m_ref[:, at] = m_new
-        pv = jnp.dot(v_t, p.astype(jnp.bfloat16), preferred_element_type=jnp.float32)
-        acc_ref[:, at] = acc_ref[:, at] * shrink + pv
-        s = following
-
-    @pl.when(step == pl.num_programs(0) - 1)
-    def _():
-        for h in range(heads):
-            at = slice(h * tokens, (h + 1) * tokens)
-            out = acc_ref[:, at] / l_ref[:, at]
-            o_ref[:, h * width : (h + 1) * width] = out.T.astype(jnp.bfloat16)
-
-
-def attention(q_t, keys_values, tokens, width):
-    length = keys_values.shape[0]
+    keys = X_SIZE * block
+
+    def attend(cls, zz):
+        both = kv_ref[cls, zz].reshape(keys, 2 * width)
+        k = both[:, :width]
+        k_twice = jnp.concatenate([k, k], 1)
+        v_t = both[:, width:].T
+
+        def scores(t):
+            return jnp.dot(
+                k_twice, qt_ref[:, t * tile : (t + 1) * tile], preferred_element_type=jnp.float32
+            )
+
+        s = scores(0)
+        for t in range(rows // tile):
+            following = scores(t + 1) if t + 1 < rows // tile else None
+            at = slice(t * tile, (t + 1) * tile)
+            m_old = m_ref[:, at]
+            m_new = jnp.maximum(m_old, jnp.max(s, 0, keepdims=True))
+            shrink = jnp.exp2(m_old - m_new)
+            p = jnp.exp2(s - m_new)
+            l_ref[:, at] = l_ref[:, at] * shrink + jnp.sum(p, 0, keepdims=True)
+            m_ref[:, at] = m_new
+            pv = jnp.dot(v_t, p.astype(jnp.bfloat16), preferred_element_type=jnp.float32)
+            acc_ref[:, at] = acc_ref[:, at] * shrink + pv
+            s = following
+
+    def slot(i, _):
+        dist = jnp.where(i < 2, 0, (i - 2) // 4 + 1)
+        turn = lax.rem(i + 2, 4)
+        ours = jnp.where((dist == 0) | (dist == 4), lax.rem(i, 2) == 0, turn < 2)
+        side = jnp.where((dist == 0) | (dist == 4), 1, lax.rem(i, 2))
+        zz = z_of(jnp.where(side == 0, -dist, dist))
+        cls = jnp.where(ours, core, 1 - core)
+
+        @pl.when(cls != core)
+        def _():
+            for xx in range(X_SIZE):
+                pltpu.make_async_remote_copy(
+                    src_ref=kv_ref.at[cls, zz, xx],
+                    dst_ref=kv_ref.at[cls, zz, xx],
+                    send_sem=tx.at[zz, xx, 4],
+                    recv_sem=rx_core.at[zz, xx],
+                    device_id={"sp": partner, "tp": lane},
+                    device_id_type=MESH,
+                ).wait_recv()
+
+        attend(cls, zz)
+        for s in range(4):
+
+            @pl.when(((i < 2) & (s // 2 == i)) | ((i >= 2) & (i < 14) & (turn == s)))
+            def _(s=s):
+                later(dist + 1, s, start, True)
+
+        @pl.when(i == 12)
+        def _():
+            for way in range(LANES - 1):
+                w_go(way).wait_recv()
+                w_pair(way).start()
+
+        return 0
+
+    lax.fori_loop(0, 16, slot, 0)
+
+    for h in range(heads):
+        at = slice(h * block, (h + 1) * block)
+        out = acc_ref[:, at] / l_ref[:, at]
+        attn_ref[lane, :, h * width : (h + 1) * width] = out.T.astype(jnp.bfloat16)
+    for way in range(LANES - 1):
+        a_go(way).start()
+    d_go(2).start()
+    w_copy.wait()
+    for way in range(LANES - 1):
+        w_pair(way).wait_recv()
+    total = jnp.dot(attn_ref[lane], out_ref[lane], preferred_element_type=jnp.float32)
+    for way in range(LANES - 1):
+        a_go(way).wait_recv()
+        total = total + jnp.dot(
+            attn_ref[froms[way]], out_ref[froms[way]], preferred_element_type=jnp.float32
+        )
+    r_copy.wait()
+    for way in range(LANES - 1):
+        r_go(way).wait_recv()
+    summed = deep_alpha * res_ref[...].reshape(LANES * lane_rows, wide).astype(jnp.float32)
+    summed = summed + total.astype(jnp.bfloat16).astype(jnp.float32)
+    normed = norm_over_lanes(summed, gain_ref[...], stat_ref, s_go, lane)
+    x_ref[...] = normed.astype(jnp.bfloat16)
+
+    i_copy.wait()
+    d_copy.wait()
+    for way in range(LANES - 1):
+        i_go(way).wait_recv()
+        d_go(way).wait_recv()
+        w_go(way).wait_send()
+        w_pair(way).wait_send()
+        r_go(way).wait_send()
+        i_go(way).wait_send()
+        d_go(way).wait_send()
+        a_go(way).wait_send()
+        s_go(way).wait_send()
+    for s in range(4):
+        first(s, ended, False)
+
+    def finish(h, _):
+        for s in range(4):
+            later(h, s, ended, False)
+        return 0
+
+    lax.fori_loop(1, 5, finish, 0)
+
+
+def norm_over_lanes(z, gain, stat_ref, s_go, lane):
+    rows, wide = z.shape
+    mean = jnp.sum(z, 1, keepdims=True) * (1.0 / wide)
+    centre = z - mean
+    m2 = jnp.sum(centre * centre, 1, keepdims=True)
+    column = lax.broadcasted_iota(jnp.int32, (rows, 128), 1)
+    both = jnp.where(column == 0, mean, m2)
+    stat_ref[lane] = both.T[:8]
+    for way in range(LANES - 1):
+        s_go(way).start()
+    for way in range(LANES - 1):
+        s_go(way).wait_recv()
+    means = [stat_ref[j][0:1] for j in range(LANES)]
+    m2s = [stat_ref[j][1:2] for j in range(LANES)]
+    full = (means[0] + means[1] + means[2] + means[3]) * (1.0 / LANES)
+    away = sum((v - full) * (v - full) for v in means)
+    spread = (m2s[0] + m2s[1] + m2s[2] + m2s[3] + wide * away) * (1.0 / (wide * LANES))
+    scale = lax.rsqrt(spread + 1e-06)
+    row = lax.broadcasted_iota(jnp.int32, (128, rows), 0)
+    packed = jnp.where(row == 0, full, scale).T
+    return (z - packed[:, 0:1]) * packed[:, 1:2] * gain
+
+
+def front(q_t, keys_values, out_weight, down_proj, resid, info, gain):
+    tokens, pair = keys_values.shape
+    width = pair // 2
     rows = q_t.shape[1]
-    block = min(KEY_BLOCK, length)
-    heads = rows // tokens
+    depth, model = out_weight.shape
+    wide = model // LANES
+    vmem = pl.BlockSpec(memory_space=pltpu.VMEM)
+    hbm = pl.BlockSpec(memory_space=pltpu.HBM)
+    dma = pltpu.SemaphoreType.DMA
+    others = LANES - 1
     return pl.pallas_call(
-        attention_kernel,
-        grid=(length // block,),
-        in_specs=[
-            pl.BlockSpec(q_t.shape, lambda i: (0, 0)),
-            pl.BlockSpec((block, width), lambda i: (i, 0)),
-            pl.BlockSpec((block, width), lambda i: (i, 1)),
+        front_kernel,
+        in_specs=[vmem, vmem, hbm, hbm, hbm, vmem, vmem],
+        out_specs=[vmem, vmem, vmem],
+        out_shape=[
+            jax.ShapeDtypeStruct((tokens, wide), jnp.bfloat16),
+            jax.ShapeDtypeStruct((LANES, down_proj.shape[0], wide), jnp.bfloat16),
+            jax.ShapeDtypeStruct((LANES, *info.shape), jnp.float32),
         ],
-        out_specs=pl.BlockSpec((tokens, heads * width), lambda i: (0, 0)),
-        out_shape=jax.ShapeDtypeStruct((tokens, heads * width), jnp.bfloat16),
         scratch_shapes=[
+            pltpu.VMEM((2, Z_SIZE, X_SIZE, tokens, pair), jnp.bfloat16),
             pltpu.VMEM((1, rows), jnp.float32),
             pltpu.VMEM((1, rows), jnp.float32),
             pltpu.VMEM((width, rows), jnp.float32),
-        ],
-        compiler_params=pltpu.CompilerParams(vmem_limit_bytes=VMEM_LIMIT),
+            pltpu.VMEM((LANES, tokens, depth), jnp.bfloat16),
+            pltpu.VMEM((LANES, depth, wide), jnp.bfloat16),
+            pltpu.VMEM((LANES, resid.shape[0], wide), jnp.bfloat16),
+            pltpu.VMEM((LANES, 8, tokens), jnp.float32),
+            dma((Z_SIZE, X_SIZE, 5)),
+            dma((Z_SIZE, X_SIZE)),
+            dma((Z_SIZE, X_SIZE, 2)),
+            dma((Z_SIZE, X_SIZE)),
+            dma((5,)),
+        ]
+        + [dma((others,))] * 14,
+        compiler_params=pltpu.CompilerParams(
+            vmem_limit_bytes=VMEM_LIMIT, collective_id=2, has_side_effects=True
+        ),
         cost_estimate=pl.CostEstimate(
-            flops=4 * rows * length * width,
-            bytes_accessed=length * width * 4,
-            transcendentals=rows * length,
+            flops=20_000_000_000, bytes_accessed=100_000_000, transcendentals=rows * 16384
         ),
-        name="attention",
-    )(q_t, keys_values, keys_values)
+        name="front",
+    )(q_t, keys_values, out_weight, down_proj, resid, info, gain)
 
 
 def half_rows(rows, columns):
@@ -470,16 +849,13 @@
     positions = lax.axis_index("sp") * tokens + jnp.arange(tokens, dtype=jnp.int32)
     rotated_keys = apply_rotary_heads(keys.reshape(tokens, 1, width), key_norm_gain, positions)
     both = jnp.concatenate([rotated_keys.reshape(tokens, width), values], 1)
-    keys_values = lax.all_gather(both, "sp", axis=0, tiled=True)
-
-    out_slice = lax.all_to_all(out_weight, "tp", split_axis=1, concat_axis=0, tiled=True)
-    down_slice = lax.all_to_all(down_proj[0], "tp", split_axis=1, concat_axis=0, tiled=True)
-    resid_slice = lax.all_to_all(resid, "tp", split_axis=1, concat_axis=0, tiled=True)
-    ids = lax.all_gather(expert_ids, "tp", axis=0, tiled=True)
     gates_own = (
         group_weight[:, None] * expert_weight / jnp.sum(expert_weight, -1, keepdims=True)
     )
-    gates = lax.all_gather(gates_own, "tp", axis=0, tiled=True)
+    top = expert_ids.shape[1]
+    info = jnp.zeros((8, own * top), jnp.float32)
+    info = info.at[0].set(expert_ids.reshape(-1).astype(jnp.float32))
+    info = info.at[1].set(gates_own.reshape(-1))
 
     q_rot = apply_rotary_heads(queries.reshape(tokens, heads, width), q_gain, positions)
     factor = np.float32(np.log2(np.e) * width**-0.5)
@@ -488,19 +864,15 @@
     fine = (scaled - coarse).astype(jnp.bfloat16)
     pair = jnp.concatenate([coarse.astype(jnp.bfloat16), fine], -1)
     q_t = pair.transpose(2, 1, 0).reshape(2 * width, heads * tokens)
-    attn = attention(q_t, keys_values, tokens, width)
-    attn = lax.all_gather(attn, "tp", axis=1, tiled=True)
-
-    proj = jnp.dot(attn, out_slice, preferred_element_type=jnp.float32)
-    proj = lax.reduce_precision(proj, 8, 7)
-    summed = deep_alpha * resid_slice.astype(jnp.float32) + proj
     gain_one = lax.dynamic_slice_in_dim(norm1_gain, lane * part, part)
     gain_two = lax.dynamic_slice_in_dim(norm2_gain, lane * part, part)
-    x_one = split_layer_norm(summed, gain_one).astype(jnp.bfloat16)
-
-    top = ids.shape[1]
+    x_one, down_slice, table = front(
+        q_t, both, out_weight, down_proj[0], resid, info, gain_one[None]
+    )
+    blocks = table[:, 0].astype(jnp.int32)
+    gates = table[:, 1].reshape(tokens, top)
+
     half = part // 2
-    blocks = ids.reshape(lanes, own * top)
     one_hot = (blocks[:, :, None] == jnp.arange(sp_count, dtype=jnp.int32)).astype(jnp.int32)
     earlier = jnp.cumsum(one_hot, 1) - one_hot
     rank = jnp.sum(earlier * one_hot, 2)
@@ -532,7 +904,9 @@
         ],
         1,
     ).astype(jnp.bfloat16)
-    returned = moe_layer(outgoing, gate_proj[0], up_proj[0], down_slice)
+    returned = moe_layer(
+        outgoing, gate_proj[0], up_proj[0], down_slice.reshape(-1, part)
+    )
 
     def weighted(pick, source):
         weights = jnp.sum(jnp.where(pick, gates[:, :, None], 0.0), 1)

time: 330 us -> 268 us (0.81)
  Pallas kernels: 146 us -> 221 us
  waiting for transfers between devices: 50.9 us -> 0 us
  blocking collectives: 60.6 us -> 22 us
  local copies, waits for them, and re-layouts: 22.3 us -> 7.25 us
  starting transfers between devices: 14 us -> 0 us
  between operations: 13.9 us -> 0.5 us
    pallas_call x1, Pallas kernels: 27.7 us -> 97.5 us  [front(): pl.pallas_call(front_kernel, in_specs=[vmem, vmem, hbm, hbm, hbm, vmem, v...]
    all_gather x2 -> x0, waiting for transfers between devices: 50.8 us -> none  [the longest x1 45.5 us: per_device(): keys_values = lax.all_gather(both, 'sp', axis=0, tiled=True)]
    all_gather x2 -> x0, blocking collectives: 21 us -> none  [the longest x1 11.3 us: per_device(): ids = lax.all_gather(expert_ids, 'tp', axis=0, tiled=True)]
    all_gather x2 -> x1, blocking collectives: 28 us -> 10.4 us  [split_layer_norm(): both = lax.all_gather(jnp.stack([mean, m2]), 'tp', axis=0, tiled=False)]
    all_to_all x3 -> x0, starting transfers between devices: 14 us -> none  [the longest x1 4.95 us: per_device(): lax.all_to_all(out_weight, 'tp', split_axis=1, concat_axis=0, tiled=True)]
    all_to_all x4 -> x0, local copies, waits for them, and re-layouts: 12.5 us -> none  [the longest x1 6.33 us: per_device(): lax.all_to_all(out_weight, 'tp', split_axis=1, concat_axis=0, tiled=True)]
    pallas_call x1, Pallas kernels: 118 us -> 124 us  [moe_layer(): pl.pallas_call(moe_kernel, in_specs=[vmem] * 4, out_specs=vmem, out_shape...]
    unnamed x18 -> x23, local copies, waits for them, and re-layouts: 7.58 us -> 1.9 us
  transfers between devices with their start and end apart: 5 -> 0, of which waited for: 2 -> 0; matrix products, arithmetic and copies ran while one was open for 9% -> 0% of each run, Pallas kernels for 8% -> 0%
where the time goes in v3:
time: 268 us
  Pallas kernels  221 us (82%)
  blocking collectives  22 us (8%)
  other arithmetic  9.76 us (4%)
  local copies, waits for them, and re-layouts  7.25 us (3%)
  matrix products  6.85 us (3%)
    pallas_call x1, Pallas kernels, moe_layer(): pl.pallas_call(moe_kernel, in_specs=[vmem] * 4, out_specs=vmem, out_shape...  124 us
    pallas_call x1, Pallas kernels, front(): pl.pallas_call(front_kernel, in_specs=[vmem, vmem, hbm, hbm, hbm, vmem, v...  97.5 us
    all_to_all x1, blocking collectives, per_device(): return lax.all_to_all(mixed, 'tp', split_axis=0, concat_axis=1, tiled=True)  11.6 us
    all_gather x1, blocking collectives, split_layer_norm(): both = lax.all_gather(jnp.stack([mean, m2]), 'tp', axis=0, tiled=False)  10.4 us

profile of v3, /device:TPU:2, one launch (start us, length us, event | category | flops | bytes accessed | tf_op | source)
XLA Modules:
  0.0 267.6 jit_solution(6376102946753514288)
XLA Ops:
  0.0 1.1 reshape.520
  1.2 0.3 multiply_reduce_fusion.1
  1.7 0.5 fusion.42
  2.2 0.3 multiply_multiply_fusion
  2.6 0.5 subtract_convert_fusion
  3.1 0.5 reduce-precision_convert_fusion.6
  3.7 0.3 maximum_bitcast_fusion
  4.0 0.6 copy.51
  4.6 0.9 copy.68
  5.8 0.1 convert_element_type.128
  6.1 0.1 reshape.518
  6.3 1.3 dynamic_slice.6
  7.6 0.6 fusion.37
  8.2 0.7 pad_maximum_fusion.4.own_ref
  9.0 0.2 scatter.9.info_ref
  9.2 0.6 copy-done.5
  9.7 97.5 %front.1 = (bf16[256,1024]{1,0:T(8,128)(2,1)}, bf16[4,256,1024]{2,1,0:T(8,128)(2,1)}, f32[4,8,128]{2,1,0:T(8,128)}) custom-call(bf16[256,1024]{1,0:T(8,128)(2,1)} %bitcast.41, bf16[256,256]{1,0:T(8,128)(2,1)} %pad_maximum_fusion.4.own_ref, bf16[512,4096]{1,0:T(8,128)(2,1)} %w_ref.1, bf16[256,4096]{1,0:T(8,128)(2,1)} %bitcast.47, bf16[64,4096]{1,0:T(8,128)(2,1)} %resid_ref.1, ...), custom_call_target="tpu_custom_call" | custom-call | flops 20000000000 | bytes 100000000 | tf_op jit(solution)/shard_map/front/pallas_call | solution.py:461
  107.3 0.8 slice_reduce_fusion.1
  108.1 0.7 fusion.56
  108.8 0.1 fusion.27
  109.0 0.3 reduce_window_sum.11
  109.3 0.2 select_reduce_fusion.3
  109.5 0.1 reduce_sum.114
  109.7 0.1 convert_element_type.133
  110.2 0.2 fusion.3
  110.4 0.5 convolution_convert_fusion
  110.9 0.4 fusion.7
  111.3 1.3 fusion.25
  112.6 0.1 broadcast_in_dim.26
  112.8 0.9 select_reduce_fusion.1
  113.7 0.4 copy-done.2
  114.1 0.3 fusion.2
  114.4 1.3 pad_maximum_fusion.out_ref
  115.7 123.7 %experts.1 = bf16[512,1536]{1,0:T(8,128)(2,1)} custom-call(bf16[512,1536]{1,0:T(8,128)(2,1)} %pad_maximum_fusion.out_ref, bf16[4096,256]{1,0:T(8,128)(2,1)} %bitcast.48, bf16[4096,256]{1,0:T(8,128)(2,1)} %bitcast.49, bf16[1024,1024]{1,0:T(8,128)(2,1)} %bitcast.50), custom_call_target="tpu_custom_call" | custom-call | flops 6442450944 | bytes 200000000 | tf_op jit(solution)/shard_map/experts/pallas_call | solution.py:777
  239.4 1.8 fusion.10
  241.2 0.4 convolution_add_fusion.1
  241.7 0.3 fusion.22
  242.0 0.3 convolution_add_fusion.6
  242.3 0.3 convolution_add_fusion.5
  242.6 0.3 fusion.23
  242.9 0.3 convolution_add_fusion.4
  243.2 0.3 convolution_add_fusion.3
  243.6 0.6 fusion.57
  244.2 0.3 multiply_reduce_fusion
  244.5 10.4 %all-gather.1 = f32[4,2,256]{2,1,0:T(2,128)S(1)} all-gather(f32[1,2,256]{2,1,0:T(2,128)S(1)} %maximum_bitcast_fusion.1), channel_id=2, replica_groups=mesh['sp'=64,'tp'=4] {'tp'}, dimensions={0}, use_global_device_ids=true | all-gather | bytes 10240 | tf_op jit(solution)/shard_map/all_gather | solution.py:814
  255.0 0.2 multiply_convert_fusion
  255.2 11.6 %all_to_all.19 = bf16[4,64,1024]{2,1,0:T(8,128)(2,1)S(1)} all-to-all(bf16[4,64,1024]{2,1,0:T(8,128)(2,1)S(1)} %bitcast.38), channel_id=1, replica_groups=mesh['sp'=64,'tp'=4] {'tp'}, dimensions={0} | all-to-all | bytes 1048576 | tf_op jit(solution)/shard_map/all_to_all | solution.py:928
  266.8 0.8 copy.67
  (50 shorter events, 1.2 us)
Async XLA Ops:
  0.0 2.2 copy-start.8
  3.6 1.9 copy-start.3
  3.6 2.0 copy-start.7
  3.6 2.3 copy-start.6
  3.6 2.3 copy-start.10
  3.7 2.5 copy-start.9
  4.0 4.2 %copy-start.4 = (bf16[256,128]{1,0:T(8,128)(2,1)S(1)}, bf16[256,128]{1,0:T(8,128)(2,1)}, u32[]{:S(2)}) copy-start(bf16[256,128]{1,0:T(8,128)(2,1)} %param.22) | copy-start | bytes 196612
  9.1 0.6 copy-start.5
  107.3 3.1 %copy-start.1 = (bf16[256,1024]{1,0:T(8,128)(2,1)S(1)}, bf16[256,1024]{1,0:T(8,128)(2,1)}, u32[]{:S(2)}) copy-start(bf16[256,1024]{1,0:T(8,128)(2,1)} %get-tuple-element.32) | copy-start | bytes 1572868
  112.8 1.2 copy-start.2
  239.4 1.8 copy-start
  243.6 11.4 %dynamic-slice-start = ((f32[4096]{0:T(1024)}, s32[]{:T(128)}), f32[1024]{0:T(1024)S(1)}, s32[]{:S(2)}) async-start(f32[4096]{0:T(1024)} %param.27, s32[]{:T(128)} %select_n.203), calls=%async_computation.1 | async-start | bytes 8704 | tf_op jit(solution)/shard_map/dynamic_slice | solution.py:868

commit v4 on v3

--- a/solution.py
+++ b/solution.py
@@ -243,48 +243,68 @@
     def later(h, s, act, wait):
         xx = x_order[s]
 
-        @pl.when(h < 4)
-        def _():
-            for side in range(2):
-                zz = z_of(-h if side == 0 else h)
-
-                @pl.when(core == 0)
-                def _():
+        @pl.when(core == 0)
+        def _():
+            @pl.when(h < 4)
+            def _():
+                for side in range(2):
+                    zz = z_of(-h if side == 0 else h)
                     if wait:
                         wait_block(zz, xx, False)
                     along_z(h, xx, side, act)
-
-                @pl.when(core == 1)
+                    act(send(core, zz, xx, 4))
+
+            @pl.when(h == 4)
+            def _():
+                zz = z_of(4)
+                if wait:
+                    wait_block(zz, xx, True)
+                act(send(core, zz, xx, 4))
+
+        @pl.when(core == 1)
+        def _():
+            if s == 0:
+
+                @pl.when(h < 4)
                 def _():
+                    ahead(h + 1, act, wait)
+            else:
+
+                @pl.when(h < 4)
+                def _():
+                    for side in range(2):
+                        zz = z_of(-h if side == 0 else h)
+                        if wait:
+                            wait_block(zz, xx, s == 3)
+                        along_x(zz, s, act)
+                        act(send(core, zz, xx, 4))
+
+                @pl.when(h == 4)
+                def _():
+                    zz = z_of(4)
                     if wait:
                         wait_block(zz, xx, s == 3)
-                    if s == 0:
-                        along_z(h, xx, side, act)
                     along_x(zz, s, act)
-
-                act(send(core, zz, xx, 4))
+                    act(send(core, zz, xx, 4))
+
+    def ahead(h, act, wait):
+        @pl.when(h < 4)
+        def _():
+            for side in range(2):
+                zz = z_of(-h if side == 0 else h)
+                if wait:
+                    wait_block(zz, x_at, False)
+                along_z(h, x_at, side, act)
+                along_x(zz, 0, act)
+                act(send(core, zz, x_at, 4))
 
         @pl.when(h == 4)
         def _():
             zz = z_of(4)
             if wait:
-                if s in (0, 3):
-                    wait_block(zz, xx, True)
-                else:
-
-                    @pl.when(core == 0)
-                    def _():
-                        wait_block(zz, xx, True)
-
-                    @pl.when(core == 1)
-                    def _():
-                        wait_block(zz, xx, False)
-
-            @pl.when(core == 1)
-            def _():
-                along_x(zz, s, act)
-
-            act(send(core, zz, xx, 4))
+                wait_block(zz, x_at, True)
+            along_x(zz, 0, act)
+            act(send(core, zz, x_at, 4))
 
     def start(copy):
         copy.start()
@@ -310,6 +330,11 @@
     r_copy.start()
     d_copy.start()
     i_copy.start()
+
+    @pl.when(core == 1)
+    def _():
+        ahead(1, start, True)
+
     for s in range(1, 4):
         first(s, start, True)
 
@@ -399,7 +424,8 @@
         r_go(way).wait_recv()
     summed = deep_alpha * res_ref[...].reshape(LANES * lane_rows, wide).astype(jnp.float32)
     summed = summed + total.astype(jnp.bfloat16).astype(jnp.float32)
-    normed = norm_over_lanes(summed, gain_ref[...], stat_ref, s_go, lane)
+    gain = gain_ref[:, pl.ds(pl.multiple_of(lane * wide, wide), wide)]
+    normed = norm_over_lanes(summed, gain, stat_ref, s_go, lane)
     x_ref[...] = normed.astype(jnp.bfloat16)
 
     i_copy.wait()
@@ -416,6 +442,10 @@
         s_go(way).wait_send()
     for s in range(4):
         first(s, ended, False)
+
+    @pl.when(core == 1)
+    def _():
+        ahead(1, ended, False)
 
     def finish(h, _):
         for s in range(4):
@@ -511,11 +541,17 @@
 
 
 def moe_kernel(
-    out_ref,
+    x1_ref,
+    table_ref,
+    gain_ref,
     wg_ref,
     wu_ref,
     wd_ref,
+    final_ref,
+    out_ref,
     ret_ref,
+    mixed_ref,
+    stat_ref,
     x_ref,
     h_ref,
     y_ref,
@@ -529,6 +565,10 @@
     hid_recv,
     back_send,
     back_recv,
+    s_send,
+    s_recv,
+    m_send,
+    m_recv,
 ):
     sp = lax.axis_index("sp")
     lane = lax.axis_index("tp")
@@ -546,7 +586,8 @@
     count = Z_SIZE
 
     def z_offset(p):
-        return jnp.where(lax.rem(p, 2) == 1, (p + 1) // 2, lax.rem(Z_SIZE - p // 2, Z_SIZE))
+        away = jnp.where(lax.rem(p, 2) == 0, p // 2 + 1, Z_SIZE - (p + 1) // 2)
+        return jnp.where(p == count - 1, 0, away)
 
     def peer(index, sign):
         p = index // peers
@@ -565,18 +606,48 @@
 
     barrier = pltpu.get_barrier_semaphore()
 
+    blocks = count * peers
+    own_index = (count - 1) * peers
+
+    def others(index, what):
+        @pl.when(index != own_index)
+        def _():
+            what(index)
+
     def greet(index, _):
-        pl.semaphore_signal(
-            barrier, inc=1, device_id={"sp": peer(index, 1), "tp": lane}, device_id_type=MESH
-        )
+        def signal(index):
+            pl.semaphore_signal(
+                barrier, inc=1, device_id={"sp": peer(index, 1), "tp": lane}, device_id_type=MESH
+            )
+
+        others(index, signal)
         return 0
 
-    lax.fori_loop(1, count * peers, greet, 0)
+    lax.fori_loop(0, blocks, greet, 0)
     for other in (left, right, far):
         pl.semaphore_signal(
             barrier, inc=1, device_id={"sp": sp, "tp": other}, device_id_type=MESH
         )
-    pl.semaphore_wait(barrier, count * peers - 1 + LANES - 1)
+    tokens = x1_ref.shape[0]
+    spots = lax.broadcasted_iota(jnp.int32, (tokens, blocks * 8), 1).astype(jnp.float32)
+
+    def pick(column):
+        return (spots == table_ref[:, column : column + 1]).astype(jnp.float32)
+
+    def placed(first, second, source):
+        return lax.dot_general(
+            (pick(first) + pick(second)).astype(jnp.bfloat16),
+            source,
+            (((0,), (0,)), ((), ())),
+            preferred_element_type=jnp.float32,
+        )
+
+    x1 = x1_ref[...]
+    out_ref[:, :wide] = placed(0, 1, x1).astype(jnp.bfloat16)
+    out_ref[:, wide:] = (placed(2, 3, x1[:, :half]) + placed(4, 5, x1[:, half:])).astype(
+        jnp.bfloat16
+    )
+    pl.semaphore_wait(barrier, blocks - 1 + LANES - 1)
 
     def go(index):
         return pltpu.make_async_remote_copy(
@@ -630,17 +701,20 @@
             device_id_type=MESH,
         )
 
+    own_rows = pl.ds(own_index * 8, 8)
     own_in = pltpu.make_async_copy(
-        out_ref.at[pl.ds(0, 8)], x_ref.at[lane, pl.ds(0, 8)], go_recv.at[0]
-    )
-    own_out = pltpu.make_async_copy(y_ref.at[pl.ds(0, 8)], ret_ref.at[pl.ds(0, 8)], back_recv.at[0])
+        out_ref.at[own_rows], x_ref.at[lane, own_rows], go_recv.at[own_index]
+    )
+    own_out = pltpu.make_async_copy(
+        y_ref.at[own_rows], ret_ref.at[own_rows], back_recv.at[own_index]
+    )
     own_in.start()
 
     def send_one(index, _):
-        go(index).start()
+        others(index, lambda i: go(i).start())
         return 0
 
-    lax.fori_loop(1, count * peers, send_one, 0)
+    lax.fori_loop(0, blocks, send_one, 0)
 
     def hidden_of(p):
         rows = group_rows(p)
@@ -691,17 +765,12 @@
     def step(t, _):
         @pl.when(t < count)
         def _():
-            @pl.when(t == 0)
+            @pl.when(t == count - 1)
             def _():
                 own_in.wait()
 
             def arrived(i, _):
-                index = t * peers + i
-
-                @pl.when(index > 0)
-                def _():
-                    go(index).wait_recv()
-
+                others(t * peers + i, lambda index: go(index).wait_recv())
                 return 0
 
             lax.fori_loop(0, peers, arrived, 0)
@@ -729,17 +798,12 @@
                 hid(t - 3, way).wait_recv()
             output_of(t - 3)
 
-            @pl.when(t == 3)
+            @pl.when(t == count + 2)
             def _():
                 own_out.start()
 
             def send_back(i, _):
-                index = (t - 3) * peers + i
-
-                @pl.when(index > 0)
-                def _():
-                    back(index).start()
-
+                others((t - 3) * peers + i, lambda index: back(index).start())
                 return 0
 
             lax.fori_loop(0, peers, send_back, 0)
@@ -750,12 +814,66 @@
     own_out.wait()
 
     def finish(index, _):
-        go(index).wait_send()
-        back(index).wait_send()
-        back(index).wait_recv()
+        def ended(index):
+            go(index).wait_send()
+            back(index).wait_send()
+            back(index).wait_recv()
+
+        others(index, ended)
         return 0
 
-    lax.fori_loop(1, count * peers, finish, 0)
+    lax.fori_loop(0, blocks, finish, 0)
+
+    moe = None
+    for k in range(2):
+
+        def chosen(column, source):
+            return jnp.dot(
+                pick(column + k).astype(jnp.bfloat16), source, preferred_element_type=jnp.float32
+            )
+
+        expert_out = chosen(0, ret_ref[:, :wide]) + jnp.concatenate(
+            [chosen(2, ret_ref[:, wide:]), chosen(4, ret_ref[:, wide:])], 1
+        )
+        term = table_ref[:, 6 + k : 7 + k] * expert_out
+        moe = term if moe is None else moe + term
+    mixed = deep_alpha * x1_ref[...].astype(jnp.float32) + moe
+    lanes_of = (right, left, far)
+
+    def s_go(way):
+        return pltpu.make_async_remote_copy(
+            src_ref=stat_ref.at[lane],
+            dst_ref=stat_ref.at[lane],
+            send_sem=s_send.at[way],
+            recv_sem=s_recv.at[way],
+            device_id={"sp": sp, "tp": lanes_of[way]},
+            device_id_type=MESH,
+        )
+
+    own_tokens = tokens // LANES
+
+    def m_go(way):
+        rows = pl.ds(pl.multiple_of(lanes_of[way] * own_tokens, own_tokens), own_tokens)
+        return pltpu.make_async_remote_copy(
+            src_ref=mixed_ref.at[rows],
+            dst_ref=final_ref.at[:, pl.ds(pl.multiple_of(lane * wide, wide), wide)],
+            send_sem=m_send.at[way],
+            recv_sem=m_recv.at[way],
+            device_id={"sp": sp, "tp": lanes_of[way]},
+            device_id_type=MESH,
+        )
+
+    gain = gain_ref[:, pl.ds(pl.multiple_of(lane * wide, wide), wide)]
+    mixed_ref[...] = norm_over_lanes(mixed, gain, stat_ref, s_go, lane).astype(jnp.bfloat16)
+    for way in range(LANES - 1):
+        m_go(way).start()
+    final_ref[:, pl.ds(pl.multiple_of(lane * wide, wide), wide)] = mixed_ref[
+        pl.ds(pl.multiple_of(lane * own_tokens, own_tokens), own_tokens)
+    ]
+    for way in range(LANES - 1):
+        s_go(way).wait_send()
+        m_go(way).wait_recv()
+        m_go(way).wait_send()
 
     def finish_group(p, _):
         for way in range(2):
@@ -768,18 +886,23 @@
     lax.fori_loop(0, count, finish_group, 0)
 
 
-def moe_layer(outgoing, w_gate, w_up, w_down):
-    rows, columns = outgoing.shape
+def moe_layer(x_one, table, gain, w_gate, w_up, w_down):
+    tokens, wide = x_one.shape
+    rows, columns = Z_SIZE * X_SIZE * 2 * 8, wide * 3 // 2
     hidden = w_gate.shape[1]
     blocks = rows // 8
     vmem = pl.BlockSpec(memory_space=pltpu.VMEM)
     dma = pltpu.SemaphoreType.DMA
     return pl.pallas_call(
         moe_kernel,
-        in_specs=[vmem] * 4,
+        in_specs=[vmem] * 6,
         out_specs=vmem,
-        out_shape=jax.ShapeDtypeStruct((rows, columns), jnp.bfloat16),
+        out_shape=jax.ShapeDtypeStruct((tokens // LANES, wide * LANES), jnp.bfloat16),
         scratch_shapes=[
+            pltpu.VMEM((rows, columns), jnp.bfloat16),
+            pltpu.VMEM((rows, columns), jnp.bfloat16),
+            pltpu.VMEM((tokens, wide), jnp.bfloat16),
+            pltpu.VMEM((LANES, 8, tokens), jnp.float32),
             pltpu.VMEM((LANES, rows, columns), jnp.bfloat16),
             pltpu.VMEM((LANES, rows, hidden * 3 // 2), jnp.bfloat16),
             pltpu.VMEM((rows, columns), jnp.bfloat16),
@@ -793,6 +916,10 @@
             dma((Z_SIZE, LANES - 1)),
             dma((blocks,)),
             dma((blocks,)),
+            dma((LANES - 1,)),
+            dma((LANES - 1,)),
+            dma((LANES - 1,)),
+            dma((LANES - 1,)),
         ],
         compiler_params=pltpu.CompilerParams(
             vmem_limit_bytes=VMEM_LIMIT, collective_id=1, has_side_effects=True
@@ -803,20 +930,7 @@
             transcendentals=0,
         ),
         name="experts",
-    )(outgoing, w_gate, w_up, w_down)
-
-
-def split_layer_norm(z, gain):
-    local = z.shape[-1]
-    mean = jnp.mean(z, -1)
-    centre = z - mean[:, None]
-    m2 = jnp.sum(centre * centre, -1)
-    both = lax.all_gather(jnp.stack([mean, m2]), "tp", axis=0, tiled=False)
-    means, m2s = both[:, 0], both[:, 1]
-    full_mean = jnp.mean(means, 0)
-    away = means - full_mean[None]
-    spread = (jnp.sum(m2s, 0) + local * jnp.sum(away * away, 0)) / (local * both.shape[0])
-    return (z - full_mean[:, None]) * lax.rsqrt(spread + 1e-06)[:, None] * gain
+    )(x_one, table, gain, w_gate, w_up, w_down)
 
 
 def per_device(
@@ -853,9 +967,26 @@
         group_weight[:, None] * expert_weight / jnp.sum(expert_weight, -1, keepdims=True)
     )
     top = expert_ids.shape[1]
-    info = jnp.zeros((8, own * top), jnp.float32)
-    info = info.at[0].set(expert_ids.reshape(-1).astype(jnp.float32))
-    info = info.at[1].set(gates_own.reshape(-1))
+    sp = lax.axis_index("sp")
+    flat = expert_ids.reshape(-1)
+    one_hot = (flat[:, None] == jnp.arange(sp_count, dtype=jnp.int32)).astype(jnp.int32)
+    earlier = jnp.cumsum(one_hot, 0) - one_hot
+    rank = jnp.sum(earlier * one_hot, 1)
+    dz = (flat // (2 * X_SIZE) - sp // (2 * X_SIZE)) % Z_SIZE
+    dx = (flat // 2 - sp // 2) % X_SIZE
+    dc = (flat - sp) % 2
+    near = jnp.where(dz <= Z_SIZE // 2, 2 * dz - 2, 2 * (Z_SIZE - dz) - 1)
+    near = jnp.where(dz == 0, Z_SIZE - 1, near)
+    target = ((near * X_SIZE + dx) * 2 + dc) * 8
+    place = lane * CAP + rank
+    row_a = jnp.where(place < 8, target + place, -1)
+    row_b = jnp.where(place < 8, -1, target + place - 8)
+    row_c = jnp.where(place < 8, -1, target + place - 4)
+    info = jnp.concatenate(
+        [v.reshape(own, top).astype(jnp.float32) for v in (row_a, row_b, row_c)]
+        + [gates_own, jnp.zeros((own, 128 - 4 * top), jnp.float32)],
+        1,
+    )
 
     q_rot = apply_rotary_heads(queries.reshape(tokens, heads, width), q_gain, positions)
     factor = np.float32(np.log2(np.e) * width**-0.5)
@@ -864,68 +995,17 @@
     fine = (scaled - coarse).astype(jnp.bfloat16)
     pair = jnp.concatenate([coarse.astype(jnp.bfloat16), fine], -1)
     q_t = pair.transpose(2, 1, 0).reshape(2 * width, heads * tokens)
-    gain_one = lax.dynamic_slice_in_dim(norm1_gain, lane * part, part)
-    gain_two = lax.dynamic_slice_in_dim(norm2_gain, lane * part, part)
     x_one, down_slice, table = front(
-        q_t, both, out_weight, down_proj[0], resid, info, gain_one[None]
-    )
-    blocks = table[:, 0].astype(jnp.int32)
-    gates = table[:, 1].reshape(tokens, top)
-
-    half = part // 2
-    one_hot = (blocks[:, :, None] == jnp.arange(sp_count, dtype=jnp.int32)).astype(jnp.int32)
-    earlier = jnp.cumsum(one_hot, 1) - one_hot
-    rank = jnp.sum(earlier * one_hot, 2)
-    sp = lax.axis_index("sp")
-    dz = (blocks // (2 * X_SIZE) - sp // (2 * X_SIZE)) % Z_SIZE
-    dx = (blocks // 2 - sp // 2) % X_SIZE
-    dc = (blocks - sp) % 2
-    near = jnp.where(dz == 0, 0, jnp.where(dz <= Z_SIZE // 2, 2 * dz - 1, 2 * (Z_SIZE - dz)))
-    target = (near * X_SIZE + dx) * 2 + dc
-    place = jnp.arange(lanes, dtype=jnp.int32)[:, None] * CAP + rank
-    row_a = jnp.where(place < 8, target * 8 + place, -1).reshape(tokens, top)
-    row_b = jnp.where(place < 8, -1, target * 8 + place - 8).reshape(tokens, top)
-    rows = jnp.arange(sp_count * 8, dtype=jnp.int32)
-    picks = (row_a[:, :, None] == rows, row_b[:, :, None] == rows, row_b[:, :, None] + 4 == rows)
-    picks = (picks[0], picks[1] & (row_b[:, :, None] >= 0), picks[2] & (row_b[:, :, None] >= 0))
-
-    def placed(pick, source):
-        return lax.dot_general(
-            jnp.any(pick, 1).astype(jnp.bfloat16),
-            source,
-            (((0,), (0,)), ((), ())),
-            preferred_element_type=jnp.float32,
-        )
-
-    outgoing = jnp.concatenate(
-        [
-            placed(picks[0], x_one),
-            placed(picks[1], x_one[:, :half]) + placed(picks[2], x_one[:, half:]),
-        ],
-        1,
-    ).astype(jnp.bfloat16)
-    returned = moe_layer(
-        outgoing, gate_proj[0], up_proj[0], down_slice.reshape(-1, part)
-    )
-
-    def weighted(pick, source):
-        weights = jnp.sum(jnp.where(pick, gates[:, :, None], 0.0), 1)
-        total = None
-        for _ in range(3):
-            term = lax.reduce_precision(weights, 8, 7)
-            weights = weights - term
-            piece = jnp.dot(
-                term.astype(jnp.bfloat16), source, preferred_element_type=jnp.float32
-            )
-            total = piece if total is None else total + piece
-        return total
-
-    moe = weighted(picks[0], returned[:, :part]) + jnp.concatenate(
-        [weighted(picks[1], returned[:, part:]), weighted(picks[2], returned[:, part:])], 1
-    )
-    final = deep_alpha * x_one.astype(jnp.float32) + moe
-    mixed = split_layer_norm(final, gain_two).astype(jnp.bfloat16)
-    return lax.all_to_all(mixed, "tp", split_axis=0, concat_axis=1, tiled=True)
+        q_t, both, out_weight, down_proj[0], resid, info, norm1_gain[None]
+    )
+    return moe_layer(
+        x_one,
+        table.reshape(tokens, -1),
+        norm2_gain[None],
+        gate_proj[0],
+        up_proj[0],
+        down_slice.reshape(-1, part),
+    )
 
 
 def solution(mesh):

time: 268 us -> 233 us (0.87)
  blocking collectives: 22 us -> 0 us
  matrix products: 6.85 us -> 0 us
  Pallas kernels: 221 us -> 217 us
    all_to_all x1 -> x0, blocking collectives: 11.6 us -> none  [per_device(): return lax.all_to_all(mixed, 'tp', split_axis=0, concat_axis=1, tiled=True)]
    all_gather x1 -> x0, blocking collectives: 10.4 us -> none  [split_layer_norm(): both = lax.all_gather(jnp.stack([mean, m2]), 'tp', axis=0, tiled=False)]
    pallas_call x1, Pallas kernels: 97.5 us -> 87.3 us  [front(): pl.pallas_call(front_kernel, in_specs=[vmem, vmem, hbm, hbm, hbm, vmem, v...]
    dot_general x12 -> x0, matrix products: 6.85 us -> none  [the longest x9 4.69 us: weighted(): jnp.dot(term.astype(jnp.bfloat16), source, preferred_element_type=jnp.flo...]
    pallas_call x1, Pallas kernels: 124 us -> 130 us  [moe_layer(): pl.pallas_call(moe_kernel, in_specs=[vmem] * 6, out_specs=vmem, out_shape...]
where the time goes in v4:
time: 233 us; the launch traced here: 232 us
  Pallas kernels  217 us (93%)
  other arithmetic  8.59 us (4%)
  local copies, waits for them, and re-layouts  5.75 us (2%)
    pallas_call x1, Pallas kernels, moe_layer(): pl.pallas_call(moe_kernel, in_specs=[vmem] * 6, out_specs=vmem, out_shape...  130 us
    pallas_call x1, Pallas kernels, front(): pl.pallas_call(front_kernel, in_specs=[vmem, vmem, hbm, hbm, hbm, vmem, v...  87.3 us

profile of v4, /device:TPU:2, one launch (start us, length us, event | category | flops | bytes accessed | tf_op | source)
XLA Modules:
  0.0 231.9 jit_solution(2467245529785748365)
XLA Ops:
  0.0 0.0 copy-start.1
  0.0 0.0 copy-start
  0.0 0.7 reduce_sum.39
  0.7 0.7 multiply_divide_fusion
  1.4 1.0 fusion.1
  2.4 0.7 broadcast_compare_fusion.1
  3.1 0.1 copy.97
  3.2 0.1 copy.89
  3.4 0.1 copy.98
  3.5 0.8 copy.83
  4.2 0.1 eq.29
  4.4 0.1 copy.94
  4.5 0.1 fusion.6
  4.5 0.2 reduce_window_sum.11
  4.7 0.2 select_reduce_fusion
  4.9 0.1 add.146
  5.0 0.1 select_convert_fusion
  5.2 0.0 copy-start.2
  5.2 0.7 concatenate.58.info_ref
  5.9 0.9 fusion.3
  6.9 0.1 fusion.11
  7.0 0.6 fusion.4
  7.6 0.0 copy-done.1
  7.6 0.7 pad_maximum_fusion.3.own_ref
  8.3 0.5 fusion.10
  8.9 0.0 copy-done
  8.9 0.2 reshape.252
  9.1 0.3 multiply_reduce_fusion
  9.5 0.0 copy-done.2
  9.5 0.3 multiply_multiply_fusion
  9.8 0.5 subtract_convert_fusion
  10.3 0.5 reduce-precision_convert_fusion
  10.8 0.3 maximum_bitcast_fusion
  11.1 0.6 copy.82
  11.8 0.9 copy.104
  12.7 87.3 %front.1 = (bf16[256,1024]{1,0:T(8,128)(2,1)}, bf16[4,256,1024]{2,1,0:T(8,128)(2,1)}, f32[4,64,128]{2,1,0:T(8,128)}) custom-call(bf16[256,1024]{1,0:T(8,128)(2,1)} %bitcast.22, bf16[256,256]{1,0:T(8,128)(2,1)} %pad_maximum_fusion.3.own_ref, bf16[512,4096]{1,0:T(8,128)(2,1)} %w_ref.1, bf16[256,4096]{1,0:T(8,128)(2,1)} %bitcast.23, ...), custom_call_target="tpu_custom_call" | custom-call | flops 20000000000 | bytes 100000000 | tf_op jit(solution)/shard_map/front/pallas_call | solution.py:491
  100.0 130.0 %experts.1 = bf16[64,4096]{1,0:T(8,128)(2,1)} custom-call(bf16[256,1024]{1,0:T(8,128)(2,1)} %get-tuple-element.8.x1_ref, f32[256,128]{1,0:T(8,128)} %bitcast.29, f32[1,4096]{1,0:T(1,128)} %bitcast.27, bf16[4096,256]{1,0:T(8,128)(2,1)} %bitcast.24, bf16[4096,256]{1,0:T(8,128)(2,1)} %bitcast.25, bf16[1024,1024]{1,0:T(8,128)(2,1)} %bitcast.28), custom_call_target="tpu_custom_call" | custom-call | flops 6442450944 | bytes 200000000 | tf_op jit(solution)/shard_map/experts/pallas_call | solution.py:896
  230.0 1.9 copy.107
  (7 shorter events, 0.1 us)
Async XLA Ops:
  0.0 7.6 %copy-start.1 = (bf16[256,128]{1,0:T(8,128)(2,1)S(1)}, bf16[256,128]{1,0:T(8,128)(2,1)}, u32[]{:S(2)}) copy-start(bf16[256,128]{1,0:T(8,128)(2,1)} %param.18) | copy-start | bytes 196612
  0.0 8.9 %copy-start = (bf16[256,512]{1,0:T(8,128)(2,1)S(1)}, bf16[256,512]{1,0:T(8,128)(2,1)}, u32[]{:S(2)}) copy-start(bf16[256,512]{1,0:T(8,128)(2,1)} %param.16) | copy-start | bytes 786436
  5.2 4.3 %copy-start.2 = (f32[128]{0:T(128)S(1)}, f32[128]{0:T(128)}, u32[]{:S(2)}) copy-start(f32[128]{0:T(128)} %param.19) | copy-start | bytes 1540

commit v5 on v4

--- a/solution.py
+++ b/solution.py
@@ -17,6 +17,7 @@
 Z_SIZE = 8
 X_SIZE = 4
 LANES = 4
+GROUPS = 16
 
 
 def apply_rotary_heads(block, gain, grid_positions):
@@ -324,7 +325,7 @@
         w_go(way).start()
     for way in range(LANES - 1):
         r_go(way).start()
-    for way in range(2):
+    for way in range(LANES - 1):
         d_go(way).start()
     w_copy.start()
     r_copy.start()
@@ -409,7 +410,6 @@
         attn_ref[lane, :, h * width : (h + 1) * width] = out.T.astype(jnp.bfloat16)
     for way in range(LANES - 1):
         a_go(way).start()
-    d_go(2).start()
     w_copy.wait()
     for way in range(LANES - 1):
         w_pair(way).wait_recv()
@@ -582,12 +582,14 @@
     half = wide // 2
     deep = wd_ref.shape[0] // LANES
     peers = X_SIZE * 2
-    group = 8 * peers
-    count = Z_SIZE
+    blocks = Z_SIZE * peers
+    count = GROUPS
+    members = blocks // count
+    group = 8 * members
 
     def z_offset(p):
         away = jnp.where(lax.rem(p, 2) == 0, p // 2 + 1, Z_SIZE - (p + 1) // 2)
-        return jnp.where(p == count - 1, 0, away)
+        return jnp.where(p == Z_SIZE - 1, 0, away)
 
     def peer(index, sign):
         p = index // peers
@@ -606,8 +608,8 @@
 
     barrier = pltpu.get_barrier_semaphore()
 
-    blocks = count * peers
-    own_index = (count - 1) * peers
+    own_index = (Z_SIZE - 1) * peers
+    own_group = own_index // members
 
     def others(index, what):
         @pl.when(index != own_index)
@@ -765,15 +767,15 @@
     def step(t, _):
         @pl.when(t < count)
         def _():
-            @pl.when(t == count - 1)
+            @pl.when(t == own_group)
             def _():
                 own_in.wait()
 
             def arrived(i, _):
-                others(t * peers + i, lambda index: go(index).wait_recv())
+                others(t * members + i, lambda index: go(index).wait_recv())
                 return 0
 
-            lax.fori_loop(0, peers, arrived, 0)
+            lax.fori_loop(0, members, arrived, 0)
             ring(t, 0).start()
             ring(t, 1).start()
 
@@ -798,15 +800,15 @@
                 hid(t - 3, way).wait_recv()
             output_of(t - 3)
 
-            @pl.when(t == count + 2)
+            @pl.when(t == own_group + 3)
             def _():
                 own_out.start()
 
             def send_back(i, _):
-                others((t - 3) * peers + i, lambda index: back(index).start())
+                others((t - 3) * members + i, lambda index: back(index).start())
                 return 0
 
-            lax.fori_loop(0, peers, send_back, 0)
+            lax.fori_loop(0, members, send_back, 0)
 
         return 0
 
@@ -908,12 +910,12 @@
             pltpu.VMEM((rows, columns), jnp.bfloat16),
             dma((blocks,)),
             dma((blocks,)),
-            dma((Z_SIZE, 2)),
-            dma((Z_SIZE, 2)),
-            dma((Z_SIZE, 2)),
-            dma((Z_SIZE, 2)),
-            dma((Z_SIZE, LANES - 1)),
-            dma((Z_SIZE, LANES - 1)),
+            dma((GROUPS, 2)),
+            dma((GROUPS, 2)),
+            dma((GROUPS, 2)),
+            dma((GROUPS, 2)),
+            dma((GROUPS, LANES - 1)),
+            dma((GROUPS, LANES - 1)),
             dma((blocks,)),
             dma((blocks,)),
             dma((LANES - 1,)),

time: 233 us -> 212 us (0.910)
  Pallas kernels: 217 us -> 197 us
    pallas_call x1, Pallas kernels: 130 us -> 114 us  [moe_layer(): pl.pallas_call(moe_kernel, in_specs=[vmem] * 6, out_specs=vmem, out_shape...]
    pallas_call x1, Pallas kernels: 87.3 us -> 82.8 us  [front(): pl.pallas_call(front_kernel, in_specs=[vmem, vmem, hbm, hbm, hbm, vmem, v...]
where the time goes in v5:
time: 212 us
  Pallas kernels  197 us (93%)
  other arithmetic  8.59 us (4%)
  local copies, waits for them, and re-layouts  5.75 us (3%)
    pallas_call x1, Pallas kernels, moe_layer(): pl.pallas_call(moe_kernel, in_specs=[vmem] * 6, out_specs=vmem, out_shape...  114 us
    pallas_call x1, Pallas kernels, front(): pl.pallas_call(front_kernel, in_specs=[vmem, vmem, hbm, hbm, hbm, vmem, v...  82.8 us

profile of v5, /device:TPU:2, one launch (start us, length us, event | category | flops | bytes accessed | tf_op | source)
XLA Modules:
  0.0 211.5 jit_solution(14945139894807260958)
XLA Ops:
  0.0 0.0 copy-start.1
  0.0 0.0 copy-start
  0.0 0.7 reduce_sum.39
  0.7 0.7 multiply_divide_fusion
  1.4 1.0 fusion.1
  2.4 0.7 broadcast_compare_fusion.1
  3.1 0.1 copy.97
  3.2 0.1 copy.89
  3.4 0.1 copy.98
  3.5 0.8 copy.83
  4.2 0.1 eq.29
  4.4 0.1 copy.94
  4.5 0.1 fusion.6
  4.5 0.2 reduce_window_sum.11
  4.7 0.2 select_reduce_fusion
  4.9 0.1 add.146
  5.0 0.1 select_convert_fusion
  5.2 0.0 copy-start.2
  5.2 0.7 concatenate.58.info_ref
  5.9 0.9 fusion.3
  6.9 0.1 fusion.11
  7.0 0.6 fusion.4
  7.6 0.0 copy-done.1
  7.6 0.7 pad_maximum_fusion.3.own_ref
  8.3 0.5 fusion.10
  8.9 0.0 copy-done
  8.9 0.2 reshape.252
  9.1 0.3 multiply_reduce_fusion
  9.5 0.0 copy-done.2
  9.5 0.3 multiply_multiply_fusion
  9.8 0.5 subtract_convert_fusion
  10.3 0.5 reduce-precision_convert_fusion
  10.8 0.3 maximum_bitcast_fusion
  11.1 0.6 copy.82
  11.8 0.9 copy.104
  12.7 82.8 %front.1 = (bf16[256,1024]{1,0:T(8,128)(2,1)}, bf16[4,256,1024]{2,1,0:T(8,128)(2,1)}, f32[4,64,128]{2,1,0:T(8,128)}) custom-call(bf16[256,1024]{1,0:T(8,128)(2,1)} %bitcast.22, bf16[256,256]{1,0:T(8,128)(2,1)} %pad_maximum_fusion.3.own_ref, bf16[512,4096]{1,0:T(8,128)(2,1)} %w_ref.1, bf16[256,4096]{1,0:T(8,128)(2,1)} %bitcast.23, ...), custom_call_target="tpu_custom_call" | custom-call | flops 20000000000 | bytes 100000000 | tf_op jit(solution)/shard_map/front/pallas_call | solution.py:491
  95.5 114.2 %experts.1 = bf16[64,4096]{1,0:T(8,128)(2,1)} custom-call(bf16[256,1024]{1,0:T(8,128)(2,1)} %get-tuple-element.8.x1_ref, f32[256,128]{1,0:T(8,128)} %bitcast.29, f32[1,4096]{1,0:T(1,128)} %bitcast.27, bf16[4096,256]{1,0:T(8,128)(2,1)} %bitcast.24, bf16[4096,256]{1,0:T(8,128)(2,1)} %bitcast.25, bf16[1024,1024]{1,0:T(8,128)(2,1)} %bitcast.28), custom_call_target="tpu_custom_call" | custom-call | flops 6442450944 | bytes 200000000 | tf_op jit(solution)/shard_map/experts/pallas_call | solution.py:898
  209.6 1.9 copy.107
  (7 shorter events, 0.1 us)
Async XLA Ops:
  0.0 7.6 %copy-start.1 = (bf16[256,128]{1,0:T(8,128)(2,1)S(1)}, bf16[256,128]{1,0:T(8,128)(2,1)}, u32[]{:S(2)}) copy-start(bf16[256,128]{1,0:T(8,128)(2,1)} %param.18) | copy-start | bytes 196612
  0.0 8.9 %copy-start = (bf16[256,512]{1,0:T(8,128)(2,1)S(1)}, bf16[256,512]{1,0:T(8,128)(2,1)}, u32[]{:S(2)}) copy-start(bf16[256,512]{1,0:T(8,128)(2,1)} %param.16) | copy-start | bytes 786436
  5.2 4.3 %copy-start.2 = (f32[128]{0:T(128)S(1)}, f32[128]{0:T(128)}, u32[]{:S(2)}) copy-start(f32[128]{0:T(128)} %param.19) | copy-start | bytes 1540

commit v6 on v5

--- a/solution.py
+++ b/solution.py
@@ -408,7 +408,7 @@
         at = slice(h * block, (h + 1) * block)
         out = acc_ref[:, at] / l_ref[:, at]
         attn_ref[lane, :, h * width : (h + 1) * width] = out.T.astype(jnp.bfloat16)
-    for way in range(LANES - 1):
+    for way in (2, 0, 1):
         a_go(way).start()
     w_copy.wait()
     for way in range(LANES - 1):
@@ -791,7 +791,7 @@
             passed(t - 2, 0).wait_recv()
             passed(t - 2, 1).wait_recv()
             hidden_of(t - 2)
-            for way in range(LANES - 1):
+            for way in (2, 0, 1):
                 hid(t - 2, way).start()
 
         @pl.when(t >= 3)
@@ -867,7 +867,7 @@
 
     gain = gain_ref[:, pl.ds(pl.multiple_of(lane * wide, wide), wide)]
     mixed_ref[...] = norm_over_lanes(mixed, gain, stat_ref, s_go, lane).astype(jnp.bfloat16)
-    for way in range(LANES - 1):
+    for way in (2, 0, 1):
         m_go(way).start()
     final_ref[:, pl.ds(pl.multiple_of(lane * wide, wide), wide)] = mixed_ref[
         pl.ds(pl.multiple_of(lane * own_tokens, own_tokens), own_tokens)

time: 212 us -> 213 us (level)
  no operation moved by 1% of the time
where the time goes in v6:
time: 213 us; the launch traced here: 212 us
  Pallas kernels  197 us (92%)
  other arithmetic  8.59 us (4%)
  local copies, waits for them, and re-layouts  5.75 us (3%)
    pallas_call x1, Pallas kernels, moe_layer(): pl.pallas_call(moe_kernel, in_specs=[vmem] * 6, out_specs=vmem, out_shape...  114 us
    pallas_call x1, Pallas kernels, front(): pl.pallas_call(front_kernel, in_specs=[vmem, vmem, hbm, hbm, hbm, vmem, v...  83.5 us

profile of v6, /device:TPU:2, one launch (start us, length us, event | category | flops | bytes accessed | tf_op | source)
XLA Modules:
  0.0 211.7 jit_solution(2579469995485246126)
XLA Ops:
  0.0 0.0 copy-start.1
  0.0 0.0 copy-start
  0.0 0.7 reduce_sum.39
  0.7 0.7 multiply_divide_fusion
  1.4 1.0 fusion.1
  2.4 0.7 broadcast_compare_fusion.1
  3.1 0.1 copy.97
  3.2 0.1 copy.89
  3.4 0.1 copy.98
  3.5 0.8 copy.83
  4.2 0.1 eq.29
  4.4 0.1 copy.94
  4.5 0.1 fusion.6
  4.5 0.2 reduce_window_sum.11
  4.7 0.2 select_reduce_fusion
  4.9 0.1 add.146
  5.0 0.1 select_convert_fusion
  5.2 0.0 copy-start.2
  5.2 0.7 concatenate.58.info_ref
  5.9 0.9 fusion.3
  6.9 0.1 fusion.11
  7.0 0.6 fusion.4
  7.6 0.0 copy-done.1
  7.6 0.7 pad_maximum_fusion.3.own_ref
  8.3 0.5 fusion.10
  8.9 0.0 copy-done
  8.9 0.2 reshape.252
  9.1 0.3 multiply_reduce_fusion
  9.5 0.0 copy-done.2
  9.5 0.3 multiply_multiply_fusion
  9.8 0.5 subtract_convert_fusion
  10.3 0.5 reduce-precision_convert_fusion
  10.8 0.3 maximum_bitcast_fusion
  11.1 0.6 copy.82
  11.8 0.9 copy.104
  12.7 83.5 %front.1 = (bf16[256,1024]{1,0:T(8,128)(2,1)}, bf16[4,256,1024]{2,1,0:T(8,128)(2,1)}, f32[4,64,128]{2,1,0:T(8,128)}) custom-call(bf16[256,1024]{1,0:T(8,128)(2,1)} %bitcast.22, bf16[256,256]{1,0:T(8,128)(2,1)} %pad_maximum_fusion.3.own_ref, bf16[512,4096]{1,0:T(8,128)(2,1)} %w_ref.1, bf16[256,4096]{1,0:T(8,128)(2,1)} %bitcast.23, ...), custom_call_target="tpu_custom_call" | custom-call | flops 20000000000 | bytes 100000000 | tf_op jit(solution)/shard_map/front/pallas_call | solution.py:491
  96.1 113.8 %experts.1 = bf16[64,4096]{1,0:T(8,128)(2,1)} custom-call(bf16[256,1024]{1,0:T(8,128)(2,1)} %get-tuple-element.8.x1_ref, f32[256,128]{1,0:T(8,128)} %bitcast.29, f32[1,4096]{1,0:T(1,128)} %bitcast.27, bf16[4096,256]{1,0:T(8,128)(2,1)} %bitcast.24, bf16[4096,256]{1,0:T(8,128)(2,1)} %bitcast.25, bf16[1024,1024]{1,0:T(8,128)(2,1)} %bitcast.28), custom_call_target="tpu_custom_call" | custom-call | flops 6442450944 | bytes 200000000 | tf_op jit(solution)/shard_map/experts/pallas_call | solution.py:898
  209.9 1.9 copy.107
  (7 shorter events, 0.1 us)
Async XLA Ops:
  0.0 7.6 %copy-start.1 = (bf16[256,128]{1,0:T(8,128)(2,1)S(1)}, bf16[256,128]{1,0:T(8,128)(2,1)}, u32[]{:S(2)}) copy-start(bf16[256,128]{1,0:T(8,128)(2,1)} %param.18) | copy-start | bytes 196612
  0.0 8.9 %copy-start = (bf16[256,512]{1,0:T(8,128)(2,1)S(1)}, bf16[256,512]{1,0:T(8,128)(2,1)}, u32[]{:S(2)}) copy-start(bf16[256,512]{1,0:T(8,128)(2,1)} %param.16) | copy-start | bytes 786436
  5.2 4.3 %copy-start.2 = (f32[128]{0:T(128)S(1)}, f32[128]{0:T(128)}, u32[]{:S(2)}) copy-start(f32[128]{0:T(128)} %param.19) | copy-start | bytes 1540
